TPU v7x, 32 devices: a whole 2x2x4 slice. The times are simulated.
32 devices in a mesh: grp: 2 (over y), fs: 4 (over z), tp: 4 (over x, core).
Axes of the slice: x: 2, y: 2, z: 4, core: 2. Of those that a mesh axis runs over, the one named last changes fastest.
Arguments:
- tokens: bfloat16 [3072, 2048], P(('grp', 'fs'), 'tp'), parts along dimension 0, may hold values from -6 to 6
- norm_gain: float32 [2048], P('fs'), may hold values from 0.1 to 1.9
- gate_weight: float32 [4, 2048, 1024], P(None, 'fs', 'tp'), may hold values from -0.125 to 0.125
- up_weight: float32 [4, 2048, 1024], P(None, 'fs', 'tp'), may hold values from -0.125 to 0.125
- down_weight: float32 [4, 2048, 1024], P(None, 'fs', 'tp'), may hold values from -0.5 to 0.5
- expert_ids: int32 [3072, 2], P(('grp', 'fs')), parts along dimension 0, may hold values from 0 to 3, as said below
- group_logits: float32 [3072, 2], P(('grp', 'fs')), parts along dimension 0, may hold values from -2.5 to 2.5
- pair_logits: float32 [3072, 2], P(('grp', 'fs')), parts along dimension 0, may hold values from -2.5 to 2.5
Outputs:
- mixed: bfloat16 [3072, 2048], P(('grp', 'fs'), 'tp'), parts along dimension 0
- gate_out: bfloat16 [8, 2048, 1024], P(('grp', 'fs'), None, 'tp'), parts along dimension 0
- up_out: bfloat16 [8, 2048, 1024], P(('grp', 'fs'), None, 'tp'), parts along dimension 0
- down_out: bfloat16 [8, 2048, 1024], P(('grp', 'fs'), None, 'tp'), parts along dimension 0
There are 2 independent parts, one for each index of `grp`. A program takes and returns all parts, laid end to end along the dimension named above; an argument that names none is the same for every part. Nothing has to cross between parts.
Inputs may be any that keep to these rules, and one draw needn't show every extreme that they name: `expert_ids`: each row names two different experts of one group: both ids lie in the same run of 2 consecutive ids.
All inputs are finite; a program needn't handle non-finite values.
Results may differ from a plain program's by a relative error of at most 0.015.
Values may be sent and summed in bfloat16 or wider, within the bound.
A program may use at most 64 MiB of HBM per device.

v0:
```python
import functools

import jax
import jax.numpy as jnp
from jax import lax
from jax.experimental import pallas as pl
from jax.experimental.pallas import tpu as pltpu
from jax.sharding import PartitionSpec as P

MESH = pl.DeviceIdType.MESH
BF16 = jnp.bfloat16
F32 = jnp.float32


def each(count, step):
    if count <= 4:
        for i in range(count):
            step(i)
    else:
        lax.fori_loop(0, count, lambda i, c: (step(i), c)[1], 0)


def exchange_kernel(
    n_grp, n_fs, n_tp, capacity,
    tokens, gain, id_rows, group_logits, pair_logits, gate_in, up_in, down_in,
    mixed, gate_out, up_out, down_out,
    out_ref, raw, cast, ret, mix, piece, hidden, own, pair_send, pair_recv, x_send, x_recv, result,
    local_sem, raw_sem, slot_s, slot_r, wz_s, wz_r, wy_s, wy_r,
    gx_s, gx_r, gd_s, gd_r, gf_s, gf_r, pr_s, pr_r, xx_s, xx_r, rt_s, rt_r,
):
    g, f, t = lax.axis_index("grp"), lax.axis_index("fs"), lax.axis_index("tp")
    n_x = n_tp // 2
    chip, core = t // 2, lax.rem(t, 2)
    partner = chip * 2 + 1 - core
    width = piece.shape[3]
    block = cast.shape[2]
    tok_rows, padded = tokens.shape[0], out_ref.shape[1]
    experts = n_fs
    share = block // n_grp

    def fs_at(k):
        return lax.rem(f + k, n_fs)

    def outward(i):
        return jnp.where(f < n_fs // 2, i + 1, n_fs - 1 - i)

    def nearest(i):
        if n_fs != 4:
            return outward(i)
        first = jnp.where(f % 2 == 0, 1, 3)
        last = jnp.where(f == 0, 3, jnp.where(f == 3, 1, 2))
        return (first, 6 - first - last, last)[i]

    def grp_at(k):
        return lax.rem(g + k, n_grp)

    def chip_at(k):
        return lax.rem(chip + k, n_x)

    def rcopy(src, dst, ssem, rsem, axis, peer):
        return pltpu.make_async_remote_copy(
            src_ref=src, dst_ref=dst, send_sem=ssem, recv_sem=rsem,
            device_id={axis: peer}, device_id_type=MESH,
        )

    raw_copies = [
        pltpu.make_async_copy(w, raw.at[m], raw_sem.at[m])
        for m, w in enumerate((gate_in, up_in, down_in))
    ]
    for copy in raw_copies:
        copy.start()

    barrier = pltpu.get_barrier_semaphore()

    def greet(axis, peer):
        pl.semaphore_signal(barrier, inc=1, device_id={axis: peer}, device_id_type=MESH)

    each(n_fs - 1, lambda i: greet("fs", fs_at(i + 1)))
    each(n_grp - 1, lambda i: greet("grp", grp_at(i + 1)))
    each(n_x - 1, lambda i: greet("tp", chip_at(i + 1) * 2 + core))
    greet("tp", partner)

    def ints(shape, axis):
        return lax.broadcasted_iota(jnp.int32, shape, axis)

    def route(ids, axis):
        shape = (experts, tok_rows) if axis == 0 else (tok_rows, experts)
        named = [(ints(shape, axis) == i).astype(F32) for i in ids]
        square = (tok_rows, tok_rows)
        earlier = (ints(square, axis) < ints(square, 1 - axis)).astype(F32).astype(BF16)
        both = (named[0] + named[1]).astype(BF16)
        pair = (both, earlier) if axis == 0 else (earlier, both)
        before = jnp.dot(*pair, preferred_element_type=F32)
        picks, kept = [], []
        for i, name in zip(ids, named):
            rank = jnp.sum(before * name, axis=axis, keepdims=True)
            kept.append(rank < capacity)
            slot = i * padded + rank.astype(jnp.int32)
            picks.append(jnp.where(rank < capacity, slot, -1))
        return picks, kept

    row_picks, _ = route([id_rows[0:1, :], id_rows[1:2, :]], 0)

    def fill(k):
        e = fs_at(k)
        slot = ints((padded, tok_rows), 0) + e * padded
        named = (slot == row_picks[0]) | (slot == row_picks[1])
        place = jnp.where(named, 1.0, 0.0).astype(BF16)
        out_ref[e] = jnp.dot(place, tokens[...], preferred_element_type=F32).astype(BF16)

    each(n_fs - 1, lambda i: fill(i + 1))
    pl.semaphore_wait(barrier, n_fs - 1 + n_grp - 1 + n_x - 1 + 1)

    weights = (
        (cast.at[0], gate_out), (cast.at[1], up_out), (cast.at[2], down_out)
    )

    def slot_copy(k, source):
        return rcopy(out_ref.at[fs_at(k)], piece.at[t, source], slot_s.at[k],
                     slot_r.at[n_fs - k], "fs", fs_at(k))

    def slot_arrival(k):
        return rcopy(out_ref.at[f], piece.at[t, fs_at(k)], slot_s.at[k], slot_r.at[k], "fs", fs_at(k))

    each(n_fs - 1, lambda i: slot_copy(outward(i), f).start())
    fill(0)
    own_slots = pltpu.make_async_copy(out_ref.at[f], piece.at[t, f], local_sem.at[3])
    own_slots.start()

    def w_rows(source, part):
        return pl.ds(source * block + part * share, share)

    def wz_copy(m, k):
        w_in, w_out = weights[m]
        return rcopy(w_in.at[fs_at(k), pl.ds(g * share, share)], w_out.at[w_rows(f, g)],
                     wz_s.at[m, k], wz_r.at[m, n_fs - k], "fs", fs_at(k))

    def wz_arrival(m, k):
        w_in, w_out = weights[m]
        return rcopy(w_in.at[fs_at(k), pl.ds(g * share, share)], w_out.at[w_rows(fs_at(k), g)],
                     wz_s.at[m, k], wz_r.at[m, k], "fs", fs_at(k))

    def wy_copy(m, k, j):
        w_out = weights[m][1]
        rows = w_rows(fs_at(k), g)
        return rcopy(w_out.at[rows], w_out.at[rows], wy_s.at[m, k, j],
                     wy_r.at[m, k, n_grp - j], "grp", grp_at(j))

    def wy_arrival(m, k, j):
        w_out = weights[m][1]
        rows = w_rows(fs_at(k), grp_at(j))
        return rcopy(w_out.at[rows], w_out.at[rows], wy_s.at[m, k, j],
                     wy_r.at[m, k, j], "grp", grp_at(j))

    own_weights = []
    for m in range(3):
        w_in, w_out = weights[m]
        raw_copies[m].wait()

        def round_block(e):
            if m < 2:
                cast[m, e] = (gain[...] * raw[m, e]).astype(BF16)
            else:
                cast[m, e] = raw[m, e].astype(BF16)

        each(n_fs, round_block)
        copy = pltpu.make_async_copy(w_in.at[f], w_out.at[pl.ds(f * block, block)], local_sem.at[m])
        copy.start()
        own_weights.append(copy)

    for m in range(3):
        each(n_fs - 1, lambda i: wz_copy(m, outward(i)).start())

    def forward(m, k):
        wz_arrival(m, k).wait_recv()
        for j in range(1, n_grp):
            wy_copy(m, k, j).start()

    def gx_copy(k, j):
        src = piece.at[t, fs_at(k)]
        return rcopy(src, src, gx_s.at[k, j], gx_r.at[k, n_x - j], "tp", chip_at(j) * 2 + core)

    def gx_arrival(k, j):
        src = piece.at[chip_at(j) * 2 + core, fs_at(k)]
        return rcopy(src, src, gx_s.at[k, j], gx_r.at[k, j], "tp", chip_at(j) * 2 + core)

    def gd_copy(k):
        src = piece.at[t, fs_at(k)]
        return rcopy(src, src, gd_s.at[k], gd_r.at[k], "tp", partner)

    def gd_arrival(k):
        src = piece.at[partner, fs_at(k)]
        return rcopy(src, src, gd_s.at[k], gd_r.at[k], "tp", partner)

    def gf_copy(k, j):
        src = piece.at[chip_at(j) * 2 + core, fs_at(k)]
        return rcopy(src, src, gf_s.at[k, j], gf_r.at[k, j], "tp", partner)

    def gf_arrival(k, j):
        src = piece.at[chip_at(j) * 2 + 1 - core, fs_at(k)]
        return rcopy(src, src, gf_s.at[k, j], gf_r.at[k, j], "tp", partner)

    def spread(k):
        for j in range(1, n_x):
            gx_copy(k, j).start()
        gd_copy(k).start()

    own_slots.wait()
    spread(0)

    id_cols = jnp.transpose(id_rows[...])
    ids = [id_cols[:, k : k + 1] for k in range(2)]
    picks, kept = route(ids, 1)
    group_exp = jnp.exp(jnp.transpose(group_logits[...]))
    group_count = group_exp.shape[1]
    low = ints(group_exp.shape, 1) * (experts // group_count)
    member = (ids[0] >= low) & (ids[0] < low + experts // group_count)
    chosen = jnp.sum(jnp.where(member, group_exp, 0.0), axis=1, keepdims=True)
    chosen = chosen / jnp.sum(group_exp, axis=1, keepdims=True)
    pair_exp = jnp.exp(jnp.transpose(pair_logits[...]))
    pair_weight = pair_exp / jnp.sum(pair_exp, axis=1, keepdims=True) * chosen
    mix_weights = [
        jnp.where(kept[k], pair_weight[:, k : k + 1], 0.0) for k in range(2)
    ]

    def blend(k):
        e = fs_at(k)
        slot = ints((tok_rows, padded), 1) + e * padded
        named = (slot == picks[0]) | (slot == picks[1])
        place = jnp.where(named, 1.0, 0.0).astype(BF16)
        weight = jnp.where(ids[0] == e, mix_weights[0], 0.0)
        weight = weight + jnp.where(ids[1] == e, mix_weights[1], 0.0)
        return jnp.dot(place, ret[e], preferred_element_type=F32) * weight

    def spread_arrived(i):
        slot_arrival(nearest(i)).wait_recv()
        spread(nearest(i))

    each(n_fs - 1, spread_arrived)

    def hand_over(k):
        for j in range(1, n_x):
            gx_arrival(k, j).wait_recv()
            gf_copy(k, j).start()

    hand_over(0)

    each(n_fs - 1, lambda i: hand_over(nearest(i)))

    for m in range(3):
        each(n_fs - 1, lambda i: forward(m, nearest(i)))

    def all_in(m):
        own_weights[m].wait()
        for j in range(1, n_grp):
            each(n_fs - 1, lambda i: wy_arrival(m, i + 1, j).wait_recv())

    all_in(0)
    all_in(1)

    def make_hidden(k):
        source = fs_at(k)
        gd_arrival(k).wait_recv()
        for j in range(1, n_x):
            gf_arrival(k, j).wait_recv()
        gate = up = None
        for p in range(n_tp):
            rows = piece[p, source]
            cols = pl.ds(p * width, width)
            gate_part = jnp.dot(rows, gate_out[cols, :], preferred_element_type=F32)
            up_part = jnp.dot(rows, up_out[cols, :], preferred_element_type=F32)
            gate = gate_part if gate is None else gate + gate_part
            up = up_part if up is None else up + up_part
        hidden[k] = (gate / (1.0 + jnp.exp(-gate)) * up).astype(BF16)

    each(n_fs, lambda i: make_hidden(i))
    all_in(2)

    def term(k, j, to_core):
        column = (chip_at(j) * 2 + to_core) * width
        rows = down_out[pl.ds(pl.multiple_of(column, width), width), :]
        return lax.dot_general(hidden[k], rows, (((1,), (1,)), ((), ())), preferred_element_type=F32)

    def pr_copy(k):
        return rcopy(pair_send.at[k], pair_recv.at[k], pr_s.at[k], pr_r.at[k], "tp", partner)

    def stage_pair(k):
        for j in range(n_x):
            pair_send[k, j] = term(k, j, 1 - core).astype(BF16)
        pr_copy(k).start()
        for j in range(n_x):
            own[k, j] = term(k, j, core)

    def xx_copy(k, j):
        return rcopy(x_send.at[k, j], x_recv.at[k, n_x - j], xx_s.at[k, j], xx_r.at[k, n_x - j],
                     "tp", chip_at(j) * 2 + core)

    def xx_arrival(k, j):
        return rcopy(x_send.at[k, j], x_recv.at[k, j], xx_s.at[k, j], xx_r.at[k, j],
                     "tp", chip_at(j) * 2 + core)

    def stage_chip(k):
        pr_copy(k).wait_recv()
        for j in range(1, n_x):
            x_send[k, j] = (own[k, j] + pair_recv[k, j].astype(F32)).astype(BF16)
            xx_copy(k, j).start()
        own[k, 0] = own[k, 0] + pair_recv[k, 0].astype(F32)

    def rt_copy(k):
        return rcopy(result.at[k], ret.at[f], rt_s.at[k], rt_r.at[n_fs - k], "fs", fs_at(k))

    def rt_arrival(k):
        return rcopy(result.at[k], ret.at[fs_at(k)], rt_s.at[k], rt_r.at[k], "fs", fs_at(k))

    def total(k):
        acc = own[k, 0]
        for j in range(1, n_x):
            xx_arrival(k, j).wait_recv()
            acc = acc + x_recv[k, j].astype(F32)
        return acc.astype(BF16)

    def stage_home(k):
        result[k] = total(k)
        rt_copy(k).start()

    def order(i):
        return lax.rem(outward(i) + n_fs, n_fs)

    stage_pair(order(0))

    def pair_and_chip(i):
        stage_pair(order(i + 1))
        stage_chip(order(i))

    each(n_fs - 1, pair_and_chip)
    stage_chip(order(n_fs - 1))
    each(n_fs - 1, lambda i: stage_home(order(i)))
    ret[f] = total(0)
    mix[...] = blend(0)

    def collect(i):
        k = nearest(i)
        rt_arrival(k).wait_recv()
        mix[...] += blend(k)

    each(n_fs - 1, collect)
    mixed[...] = mix[...].astype(BF16)

    def drain_peer(i):
        k = i + 1
        slot_copy(k, f).wait_send()
        rt_copy(k).wait_send()
        for m in range(3):
            wz_copy(m, k).wait_send()
            for j in range(1, n_grp):
                wy_copy(m, k, j).wait_send()

    def drain_chunk(k):
        gd_copy(k).wait_send()
        pr_copy(k).wait_send()
        for j in range(1, n_x):
            gx_copy(k, j).wait_send()
            gf_copy(k, j).wait_send()
            xx_copy(k, j).wait_send()

    each(n_fs - 1, drain_peer)
    each(n_fs, drain_chunk)


def body(
    tokens, norm_gain, gate_weight, up_weight, down_weight, expert_ids, group_logits, pair_logits
):
    n_grp, n_fs, n_tp = (lax.axis_size(a) for a in ("grp", "fs", "tp"))
    n_x = n_tp // 2
    experts, block, hid = gate_weight.shape
    tok_rows, width = tokens.shape
    capacity = 5 * tok_rows * 2 // (4 * experts)
    cap = -(-capacity // 16) * 16
    vmem = pl.BlockSpec(memory_space=pltpu.VMEM)
    hbm = pl.BlockSpec(memory_space=pl.ANY)
    dma = pltpu.SemaphoreType.DMA
    matrix = jax.ShapeDtypeStruct((n_fs * block, hid), BF16)
    chunk = (n_fs, n_x, cap, width)
    sem_shapes = [
        (4,), (3,), (n_fs,), (n_fs,), (3, n_fs), (3, n_fs), (3, n_fs, n_grp), (3, n_fs, n_grp),
        (n_fs, n_x), (n_fs, n_x), (n_fs,), (n_fs,), (n_fs, n_x), (n_fs, n_x),
        (n_fs,), (n_fs,), (n_fs, n_x), (n_fs, n_x), (n_fs,), (n_fs,),
    ]
    mixed, *matrices = pl.pallas_call(
        functools.partial(exchange_kernel, n_grp, n_fs, n_tp, capacity),
        out_shape=(jax.ShapeDtypeStruct((tok_rows, width), BF16), matrix, matrix, matrix),
        in_specs=[vmem] * 5 + [hbm] * 3,
        out_specs=(vmem,) * 4,
        scratch_shapes=[
            pltpu.VMEM((n_fs, cap, width), BF16),
            pltpu.VMEM((3, n_fs, block, hid), F32),
            pltpu.VMEM((3, n_fs, block, hid), BF16),
            pltpu.VMEM((n_fs, cap, width), BF16),
            pltpu.VMEM((tok_rows, width), F32),
            pltpu.VMEM((n_tp, n_fs, cap, width), BF16),
            pltpu.VMEM((n_fs, cap, hid), BF16),
            pltpu.VMEM(chunk, F32),
            pltpu.VMEM(chunk, BF16),
            pltpu.VMEM(chunk, BF16),
            pltpu.VMEM(chunk, BF16),
            pltpu.VMEM(chunk, BF16),
            pltpu.VMEM((n_fs, cap, width), BF16),
        ] + [dma(s) for s in sem_shapes],
        compiler_params=pltpu.CompilerParams(
            collective_id=0, has_side_effects=True, vmem_limit_bytes=48 * 1024 * 1024
        ),
    )(
        tokens, norm_gain[:, None], expert_ids.T, group_logits.T, pair_logits.T,
        gate_weight, up_weight, down_weight,
    )
    return (mixed, *(m[None] for m in matrices))


def solution(mesh):
    placed = (
        P(("grp", "fs"), "tp"),
        P("fs"),
        P(None, "fs", "tp"),
        P(None, "fs", "tp"),
        P(None, "fs", "tp"),
        P(("grp", "fs"), None),
        P(("grp", "fs"), None),
        P(("grp", "fs"), None),
    )
    return jax.shard_map(
        body,
        mesh=mesh,
        in_specs=placed,
        out_specs=(
            P(("grp", "fs"), "tp"),
            P(("grp", "fs"), None, "tp"),
            P(("grp", "fs"), None, "tp"),
            P(("grp", "fs"), None, "tp"),
        ),
        check_vma=False,
    )
```

profile of v0, /device:TPU:0, one launch (start us, length us, event | category | flops | bytes accessed | tf_op | source)
XLA Modules:
  0.0 112.1 jit_solution(13677565775381111622)
XLA Ops:
  0.6 0.8 copy.12.gain
  1.5 0.0 copy-start
  1.5 1.0 copy-done
  2.5 0.0 copy-start.1
  2.5 0.7 copy-done.1
  3.1 0.0 copy-start.2
  3.1 0.7 copy-done.2
  3.8 0.0 copy-start.3
  3.8 0.7 copy-done.3
  4.5 103.9 %shard_map.111 = (bf16[384,512]{1,0:T(8,128)(2,1)S(1)}, bf16[2048,256]{1,0:T(8,128)(2,1)S(1)}, bf16[2048,256]{1,0:T(8,128)(2,1)S(1)}, bf16[2048,256]{1,0:T(8,128)(2,1)S(1)}) custom-call(bf16[384,512]{1,0:T(8,128)(2,1)S(1)} %copy-done, f32[512,1]{1,0:T(8,128)S(1)} %copy.12.gain, s32[2,384]{1,0:T(2,128)S(1)} %bitcast.10, f32[2,384]{1,0:T(2,128)S(1)} %bitcast.11, ...), custom_call_target="tpu_custom_call" | custom-call | tf_op jit(solution)/shard_map/pallas_call | solution.py:389
  108.4 0.7 copy.17
  109.2 1.0 copy.18
  110.2 1.0 copy.19
  111.1 1.0 copy.20
Async XLA Ops:
  1.5 1.0 copy-start
  2.5 0.7 copy-start.1
  3.1 0.7 copy-start.2
  3.8 0.7 copy-start.3
where the time goes:
time: 112 us
  Pallas kernels  104 us (93%)
  local copies, waits for them, and re-layouts  7.52 us (7%)
    pallas_call x1, Pallas kernels, body(): pl.pallas_call(functools.partial(exchange_kernel, n_grp, n_fs, n_tp, capa...  104 us
    unnamed x12, local copies, waits for them, and re-layouts  6.7 us

commit v1 on v0

--- a/solution.py
+++ b/solution.py
@@ -416,6 +416,473 @@
     return (mixed, *(m[None] for m in matrices))
 
 
+def pair_kernel(
+    n_grp, n_fs, n_tp, capacity,
+    tokens_in, gain_in, ids_in, group_in, pair_in, gate_in, up_in, down_in,
+    mixed, gate_out, up_out, down_out,
+    tokens, gain, id_rows, group_logits, pair_logits, gain_col,
+    raw_own, raw_far, cast, slots, place, back_place, wsend, wrecv, wcol,
+    piece, acc, hid, dwn, part_send, part_recv, keep, home_send, home, own_home, mix,
+    in_sem, raw_sem,
+    sl_s, sl_r, wm_s, wm_r, wz_s, wz_r, wy_s, wy_r, tx_s, tx_r, td_s, td_r, tf_s, tf_r,
+    dw_s, dw_r, hx_s, hx_r, hd_s, hd_r, hf_s, hf_r, pt_s, pt_r, hm_s, hm_r,
+):
+    g, f, t = lax.axis_index("grp"), lax.axis_index("fs"), lax.axis_index("tp")
+    cap, width = piece.shape[2], piece.shape[3]
+    block, hidden_units = raw_own.shape[1], raw_own.shape[2]
+    share = raw_far.shape[2]
+    tok_rows = tokens.shape[0]
+    lanes = place.shape[1]
+    pair = n_fs // 2
+
+    def flip(i, k):
+        return (i, i + 1 - 2 * lax.rem(i, 2), lax.rem(i + 2, 4), 3 - i)[k]
+
+    def fs_at(k):
+        return flip(f, k)
+
+    def tp_at(j):
+        return flip(t, j)
+
+    other_grp = 1 - g
+
+    def rcopy(src, dst, ssem, rsem, axis, peer):
+        return pltpu.make_async_remote_copy(
+            src_ref=src, dst_ref=dst, send_sem=ssem, recv_sem=rsem,
+            device_id={axis: peer}, device_id_type=MESH,
+        )
+
+    small = [
+        pltpu.make_async_copy(src, dst, in_sem.at[i])
+        for i, (src, dst) in enumerate((
+            (ids_in, id_rows), (tokens_in, tokens), (gain_in, gain),
+            (group_in, group_logits), (pair_in, pair_logits),
+        ))
+    ]
+    w_in = (gate_in, up_in, down_in)
+    w_out = (gate_out, up_out, down_out)
+
+    def far_load(m, k):
+        return pltpu.make_async_copy(
+            w_in[m].at[fs_at(k), pl.ds(g * share, share)], raw_far.at[m, k - 1], raw_sem.at[m, k]
+        )
+
+    def own_load(m):
+        return pltpu.make_async_copy(w_in[m].at[f], raw_own.at[m], raw_sem.at[m, 0])
+
+    for copy in small:
+        copy.start()
+    for m in (2, 0, 1):
+        for k in (1, 2, 3):
+            far_load(m, k).start()
+    for m in (2, 0, 1):
+        own_load(m).start()
+
+    barrier = pltpu.get_barrier_semaphore()
+
+    def greet(axis, peer):
+        pl.semaphore_signal(barrier, inc=1, device_id={axis: peer}, device_id_type=MESH)
+
+    for k in (1, 2, 3):
+        greet("fs", fs_at(k))
+        greet("tp", tp_at(k))
+    greet("grp", other_grp)
+
+    def ints(shape, axis):
+        return lax.broadcasted_iota(jnp.int32, shape, axis)
+
+    own_base = (f - lax.rem(f, 2))
+    far_base = lax.rem(own_base + 2, 4)
+    bases = (own_base, far_base)
+
+    small[0].wait()
+    first, second = id_rows[0:1, :], id_rows[1:2, :]
+    members = [(first >= b) & (first < b + 2) for b in bases]
+    square = (tok_rows, tok_rows)
+    earlier = (ints(square, 0) < ints(square, 1)).astype(F32).astype(BF16)
+    named = jnp.where(ints((8, tok_rows), 0) < 4, members[0].astype(F32), members[1].astype(F32))
+    before = jnp.dot(named.astype(BF16), earlier, preferred_element_type=F32)
+    ranks = [before[0:1, :], before[4:5, :]]
+    kept = [m & (r < capacity) for m, r in zip(members, ranks)]
+    seat = [jnp.where(k, r.astype(jnp.int32), -1) for k, r in zip(kept, ranks)]
+
+    small[1].wait()
+
+    def fill(i):
+        one_hot = jnp.where(ints((lanes, tok_rows), 0) == seat[i], 1.0, 0.0)
+        place[i] = one_hot.astype(BF16)
+        rows = jnp.dot(place[i, 0:cap, :], tokens[...], preferred_element_type=F32).astype(BF16)
+        slots[i] = rows
+        return rows
+
+    def slot_copy(k):
+        src = slots.at[0] if k == 1 else slots.at[1]
+        return rcopy(src, piece.at[t, k], sl_s.at[k], sl_r.at[k], "fs", fs_at(k))
+
+    def relay_copy():
+        return rcopy(piece.at[t, 2], piece.at[t, 3], sl_s.at[3], sl_r.at[3], "fs", fs_at(1))
+
+    fill(1)
+    pl.semaphore_wait(barrier, 3 + 3 + 1)
+    slot_copy(2).start()
+    piece[t, 0] = fill(0)
+    slot_copy(1).start()
+
+    def tx_copy(k):
+        src = piece.at[t, k]
+        return rcopy(src, src, tx_s.at[k], tx_r.at[k], "tp", tp_at(2))
+
+    def td_copy(k):
+        src = piece.at[t, k]
+        return rcopy(src, src, td_s.at[k], td_r.at[k], "tp", tp_at(1))
+
+    def tf_copy(k):
+        src = piece.at[tp_at(2), k]
+        return rcopy(src, src, tf_s.at[k], tf_r.at[k], "tp", tp_at(1))
+
+    def tx_arrival(k):
+        src = piece.at[tp_at(2), k]
+        return rcopy(src, src, tx_s.at[k], tx_r.at[k], "tp", tp_at(2))
+
+    def td_arrival(k):
+        src = piece.at[tp_at(1), k]
+        return rcopy(src, src, td_s.at[k], td_r.at[k], "tp", tp_at(1))
+
+    def tf_arrival(k):
+        src = piece.at[tp_at(3), k]
+        return rcopy(src, src, tf_s.at[k], tf_r.at[k], "tp", tp_at(1))
+
+    def spread(k):
+        tx_copy(k).start()
+        td_copy(k).start()
+
+    spread(0)
+
+    def w_rows(source, part):
+        return pl.ds(source * block + part * share, share)
+
+    def wz_copy(m, k):
+        return rcopy(cast.at[m, k - 1], w_out[m].at[w_rows(f, g)],
+                     wz_s.at[m, k], wz_r.at[m, k], "fs", fs_at(k))
+
+    def wz_arrival(m, k):
+        return rcopy(cast.at[m, k - 1], w_out[m].at[w_rows(fs_at(k), g)],
+                     wz_s.at[m, k], wz_r.at[m, k], "fs", fs_at(k))
+
+    def wy_copy(m, k):
+        rows = w_out[m].at[w_rows(fs_at(k), g)]
+        return rcopy(rows, rows, wy_s.at[m, k], wy_r.at[m, k], "grp", other_grp)
+
+    def wy_arrival(m, k):
+        rows = w_out[m].at[w_rows(fs_at(k), other_grp)]
+        return rcopy(rows, rows, wy_s.at[m, k], wy_r.at[m, k], "grp", other_grp)
+
+    small[2].wait()
+    gain_col[...] = jnp.transpose(jnp.broadcast_to(gain[...], (8, block)))[:, 0:1]
+    far_gain = gain_col[pl.ds(g * share, share), :]
+
+    def send_far(m, k):
+        far_load(m, k).wait()
+        values = raw_far[m, k - 1]
+        if m < 2:
+            values = far_gain * values
+        cast[m, k - 1] = values.astype(BF16)
+        wz_copy(m, k).start()
+
+    def round_own(m):
+        own_load(m).wait()
+        values = raw_own[m]
+        if m < 2:
+            values = gain_col[...] * values
+        w_out[m][pl.ds(f * block, block), :] = values.astype(BF16)
+
+    for k in (1, 2, 3):
+        send_far(2, k)
+    for m in (0, 1):
+        send_far(m, 1)
+
+    small[3].wait()
+    small[4].wait()
+    group_exp = jnp.exp(group_logits[...])
+    group_sum = jnp.sum(group_exp, axis=0, keepdims=True)
+    pair_exp = jnp.exp(pair_logits[...])
+    pair_weight = pair_exp / jnp.sum(pair_exp, axis=0, keepdims=True)
+    group_count = group_exp.shape[0]
+
+    def wm_copy(k):
+        return rcopy(wsend.at[k // 2], wrecv.at[k], wm_s.at[k], wm_r.at[k], "fs", fs_at(k))
+
+    chosen = jnp.zeros_like(group_sum)
+    for i in range(group_count):
+        chosen = chosen + jnp.where((first >= 2 * i) & (first < 2 * i + 2), group_exp[i : i + 1, :], 0.0)
+    mix_weight = pair_weight * (chosen / group_sum)
+    for i in range(2):
+        expert = bases[i] + ints((8, tok_rows), 0)
+        rest = jnp.where(first == expert, mix_weight[0:1, :], 0.0)
+        rest = rest + jnp.where(second == expert, mix_weight[1:2, :], 0.0)
+        total = None
+        for _ in range(3):
+            head = rest.astype(BF16)
+            rest = rest - head.astype(F32)
+            term = lax.dot_general(head, place[i], (((1,), (1,)), ((), ())), preferred_element_type=F32)
+            total = term if total is None else total + term
+        wsend[i] = total
+    for k in (1, 2, 3):
+        wm_copy(k).start()
+
+    for i in range(2):
+        back_place[i] = jnp.transpose(place[i].astype(F32))[:, 0:cap].astype(BF16)
+
+    def seat_weights(k, rows):
+        cols = jnp.transpose(rows)
+        wcol[k] = jnp.where(lax.rem(f, 2) == 0, cols[0:cap, 0:1], cols[0:cap, 1:2])
+
+    seat_weights(0, wsend[0])
+    round_own(2)
+
+    def slot_arrival(k):
+        return rcopy(slots.at[0], piece.at[t, k], sl_s.at[k], sl_r.at[k], "fs", fs_at(k))
+
+    slot_arrival(2).wait_recv()
+    relay_copy().start()
+    spread(2)
+    for k in (2, 3):
+        for m in (0, 1):
+            send_far(m, k)
+    for m in (0, 1):
+        round_own(m)
+    slot_arrival(1).wait_recv()
+    spread(1)
+
+    def hand_over(k):
+        tx_arrival(k).wait_recv()
+        tf_copy(k).start()
+
+    hand_over(0)
+    for k in (1, 2, 3):
+        wz_arrival(2, k).wait_recv()
+        wy_copy(2, k).start()
+    hand_over(2)
+    hand_over(1)
+    slot_arrival(3).wait_recv()
+    spread(3)
+
+    def dw_copy(j):
+        src = down_out.at[pl.ds(tp_at(j) * block, block)]
+        return rcopy(src, dwn.at[j], dw_s.at[j], dw_r.at[j], "tp", tp_at(j))
+
+    for k in (1, 2, 3):
+        wy_arrival(2, k).wait_recv()
+    for j in (1, 2, 3):
+        dw_copy(j).start()
+    for k in (1, 2, 3):
+        wm_copy(k).wait_recv()
+        seat_weights(k, wrecv[k])
+
+    for m in (0, 1):
+        wz_arrival(m, 1).wait_recv()
+        wy_copy(m, 1).start()
+    hand_over(3)
+    for k in (0, 2, 1, 3):
+        td_arrival(k).wait_recv()
+        tf_arrival(k).wait_recv()
+
+    def products(k, source):
+        rows = piece[source, k]
+        cols = pl.ds(source * block, block)
+        gate = jnp.dot(rows, gate_out[cols, :], preferred_element_type=F32)
+        up = jnp.dot(rows, up_out[cols, :], preferred_element_type=F32)
+        return gate, up
+
+    def first_products(k, c):
+        gate, up = products(k, f)
+        acc[0, k], acc[1, k] = gate, up
+        return c
+
+    def more_products(kk):
+        def step(k, c):
+            gate, up = products(k, fs_at(kk))
+            acc[0, k] += gate
+            acc[1, k] += up
+            return c
+        return step
+
+    lax.fori_loop(0, n_fs, first_products, 0)
+    for m in (0, 1):
+        wz_arrival(m, 2).wait_recv()
+        wy_copy(m, 2).start()
+    for m in (0, 1):
+        wy_arrival(m, 1).wait_recv()
+    lax.fori_loop(0, n_fs, more_products(1), 0)
+    for m in (0, 1):
+        wz_arrival(m, 3).wait_recv()
+        wy_copy(m, 3).start()
+    for m in (0, 1):
+        wy_arrival(m, 2).wait_recv()
+    lax.fori_loop(0, n_fs, more_products(2), 0)
+    for m in (0, 1):
+        wy_arrival(m, 3).wait_recv()
+
+    def h_copy(j, k, ssem, rsem, source):
+        return rcopy(hid.at[source, k], hid.at[source ^ j, k], ssem.at[k], rsem.at[k], "tp", tp_at(j))
+
+    def hx_copy(k):
+        return h_copy(2, k, hx_s, hx_r, 0)
+
+    def hd_copy(k):
+        return h_copy(1, k, hd_s, hd_r, 0)
+
+    def hf_copy(k):
+        return h_copy(1, k, hf_s, hf_r, 2)
+
+    order = (3, 2, 1, 0)
+    for k in order:
+        gate, up = products(k, fs_at(3))
+        gate = acc[0, k] + gate
+        up = acc[1, k] + up
+        hid[0, k] = (gate / (1.0 + jnp.exp(-gate)) * up * wcol[k]).astype(BF16)
+        hx_copy(k).start()
+        hd_copy(k).start()
+
+    for j in (1, 2, 3):
+        dw_copy(j).wait_recv()
+
+    def pass_on(k):
+        hx_copy(k).wait_recv()
+        hf_copy(k).start()
+
+    def result(k):
+        hd_copy(k).wait_recv()
+        hf_copy(k).wait_recv()
+        total = None
+        for j in range(n_tp):
+            rows = down_out[pl.ds(t * block, block), :] if j == 0 else dwn[j]
+            term = lax.dot_general(hid[j, k], rows, (((1,), (1,)), ((), ())), preferred_element_type=F32)
+            total = term if total is None else total + term
+        return total
+
+    def part_copy(i):
+        return rcopy(part_send.at[i], part_recv.at[i], pt_s.at[i], pt_r.at[i], "fs", fs_at(1))
+
+    def home_copy():
+        return rcopy(home_send, home, hm_s.at[0], hm_r.at[0], "fs", fs_at(2))
+
+    pass_on(3)
+    part_send[0] = result(3).astype(BF16)
+    part_copy(0).start()
+    pass_on(2)
+    keep[...] = result(2)
+    pass_on(1)
+    part_send[1] = result(1).astype(BF16)
+    part_copy(0).wait_recv()
+    home_send[...] = (keep[...] + part_recv[0].astype(F32)).astype(BF16)
+    home_copy().start()
+    part_copy(1).start()
+    pass_on(0)
+    keep[...] = result(0)
+    part_copy(1).wait_recv()
+    own_home[...] = (keep[...] + part_recv[1].astype(F32)).astype(BF16)
+    mix[...] = jnp.dot(back_place[0], own_home[...], preferred_element_type=F32)
+    home_copy().wait_recv()
+    far = jnp.dot(back_place[1], home[...], preferred_element_type=F32)
+    mixed[...] = (mix[...] + far).astype(BF16)
+
+    for k in (1, 2):
+        slot_copy(k).wait_send()
+    relay_copy().wait_send()
+    for k in (1, 2, 3):
+        wm_copy(k).wait_send()
+        dw_copy(k).wait_send()
+        for m in range(3):
+            wz_copy(m, k).wait_send()
+            wy_copy(m, k).wait_send()
+    for k in range(n_fs):
+        tx_copy(k).wait_send()
+        td_copy(k).wait_send()
+        tf_copy(k).wait_send()
+        hx_copy(k).wait_send()
+        hd_copy(k).wait_send()
+        hf_copy(k).wait_send()
+    for i in range(2):
+        part_copy(i).wait_send()
+    home_copy().wait_send()
+
+
+def pair_body(
+    tokens, norm_gain, gate_weight, up_weight, down_weight, expert_ids, group_logits, pair_logits
+):
+    n_grp, n_fs, n_tp = (lax.axis_size(a) for a in ("grp", "fs", "tp"))
+    experts, block, hid = gate_weight.shape
+    tok_rows, width = tokens.shape
+    share = block // n_grp
+    capacity = 5 * tok_rows * 2 // (4 * experts)
+    cap = -(-capacity // 16) * 16
+    lanes = -(-cap // 128) * 128
+    vmem = pl.BlockSpec(memory_space=pltpu.VMEM)
+    hbm = pl.BlockSpec(memory_space=pl.ANY)
+    dma = pltpu.SemaphoreType.DMA
+    matrix = jax.ShapeDtypeStruct((n_fs * block, hid), BF16)
+    rows = (cap, width)
+    sem_shapes = [
+        (5,), (3, n_fs),
+        (n_fs,), (n_fs,), (n_fs,), (n_fs,), (3, n_fs), (3, n_fs), (3, n_fs), (3, n_fs),
+        (n_fs,), (n_fs,), (n_fs,), (n_fs,), (n_fs,), (n_fs,),
+        (n_tp,), (n_tp,), (n_fs,), (n_fs,), (n_fs,), (n_fs,), (n_fs,), (n_fs,),
+        (2,), (2,), (1,), (1,),
+    ]
+    mixed, *matrices = pl.pallas_call(
+        functools.partial(pair_kernel, n_grp, n_fs, n_tp, capacity),
+        out_shape=(jax.ShapeDtypeStruct((tok_rows, width), BF16), matrix, matrix, matrix),
+        in_specs=[hbm] * 8,
+        out_specs=(vmem,) * 4,
+        scratch_shapes=[
+            pltpu.VMEM((tok_rows, width), BF16),
+            pltpu.VMEM((1, block), F32),
+            pltpu.VMEM((2, tok_rows), jnp.int32),
+            pltpu.VMEM((group_logits.shape[1], tok_rows), F32),
+            pltpu.VMEM((2, tok_rows), F32),
+            pltpu.VMEM((block, 1), F32),
+            pltpu.VMEM((3, block, hid), F32),
+            pltpu.VMEM((3, n_fs - 1, share, hid), F32),
+            pltpu.VMEM((3, n_fs - 1, share, hid), BF16),
+            pltpu.VMEM((2, *rows), BF16),
+            pltpu.VMEM((2, lanes, tok_rows), BF16),
+            pltpu.VMEM((2, tok_rows, cap), BF16),
+            pltpu.VMEM((2, 8, lanes), F32),
+            pltpu.VMEM((n_fs, 8, lanes), F32),
+            pltpu.VMEM((n_fs, cap, 1), F32),
+            pltpu.VMEM((n_tp, n_fs, *rows), BF16),
+            pltpu.VMEM((2, n_fs, cap, hid), F32),
+            pltpu.VMEM((n_tp, n_fs, cap, hid), BF16),
+            pltpu.VMEM((n_tp, block, hid), BF16),
+            pltpu.VMEM((2, *rows), BF16),
+            pltpu.VMEM((2, *rows), BF16),
+            pltpu.VMEM(rows, F32),
+            pltpu.VMEM(rows, BF16),
+            pltpu.VMEM(rows, BF16),
+            pltpu.VMEM(rows, BF16),
+            pltpu.VMEM((tok_rows, width), F32),
+        ] + [dma(s) for s in sem_shapes],
+        compiler_params=pltpu.CompilerParams(
+            collective_id=0, has_side_effects=True, vmem_limit_bytes=56 * 1024 * 1024
+        ),
+    )(
+        tokens, norm_gain[None, :], expert_ids.T, group_logits.T, pair_logits.T,
+        gate_weight, up_weight, down_weight,
+    )
+    return (mixed, *(m[None] for m in matrices))
+
+
+def paired(mesh, tokens, gate_weight, expert_ids, group_logits):
+    n_grp, n_fs, n_tp = (mesh.shape[a] for a in ("grp", "fs", "tp"))
+    experts, features, _ = gate_weight.shape
+    return (
+        experts // group_logits.shape[1] == expert_ids.shape[1] == 2
+        and n_fs == n_tp == experts == 4
+        and n_grp == 2
+    )
+
+
 def solution(mesh):
     placed = (
         P(("grp", "fs"), "tp"),
@@ -427,15 +894,21 @@
         P(("grp", "fs"), None),
         P(("grp", "fs"), None),
     )
-    return jax.shard_map(
-        body,
-        mesh=mesh,
-        in_specs=placed,
-        out_specs=(
-            P(("grp", "fs"), "tp"),
-            P(("grp", "fs"), None, "tp"),
-            P(("grp", "fs"), None, "tp"),
-            P(("grp", "fs"), None, "tp"),
-        ),
-        check_vma=False,
-    )
+
+    def run(tokens, norm_gain, gate_weight, up_weight, down_weight, expert_ids, group_logits, pair_logits):
+        args = (tokens, norm_gain, gate_weight, up_weight, down_weight, expert_ids, group_logits, pair_logits)
+        special = paired(mesh, tokens, gate_weight, expert_ids, group_logits)
+        return jax.shard_map(
+            pair_body if special else body,
+            mesh=mesh,
+            in_specs=placed,
+            out_specs=(
+                P(("grp", "fs"), "tp"),
+                P(("grp", "fs"), None, "tp"),
+                P(("grp", "fs"), None, "tp"),
+                P(("grp", "fs"), None, "tp"),
+            ),
+            check_vma=False,
+        )(*args)
+
+    return run

time: 112 us -> 102 us (0.911)
  Pallas kernels: 104 us -> 95.3 us
  local copies, waits for them, and re-layouts: 7.52 us -> 6.15 us
    pallas_call x1, Pallas kernels: 104 us -> 95.3 us  [pair_body(): pl.pallas_call(functools.partial(pair_kernel, n_grp, n_fs, n_tp, capacity...]
    unnamed x12 -> x8, local copies, waits for them, and re-layouts: 6.7 us -> 6.15 us
where the time goes in v1:
time: 102 us
  Pallas kernels  95.3 us (93%)
  local copies, waits for them, and re-layouts  6.15 us (6%)
    pallas_call x1, Pallas kernels, pair_body(): pl.pallas_call(functools.partial(pair_kernel, n_grp, n_fs, n_tp, capacity...  95.3 us
    unnamed x8, local copies, waits for them, and re-layouts  6.15 us

profile of v1, /device:TPU:0, one launch (start us, length us, event | category | flops | bytes accessed | tf_op | source)
XLA Modules:
  0.0 102.1 jit_solution(14042450573485350835)
XLA Ops:
  0.6 95.3 %shard_map.111 = (bf16[384,512]{1,0:T(8,128)(2,1)}, bf16[2048,256]{1,0:T(8,128)(2,1)}, bf16[2048,256]{1,0:T(8,128)(2,1)}, bf16[2048,256]{1,0:T(8,128)(2,1)}) custom-call(bf16[384,512]{1,0:T(8,128)(2,1)} %tokens_in.1, f32[1,512]{1,0:T(1,128)} %bitcast.13, s32[2,384]{1,0:T(2,128)} %bitcast.10, f32[2,384]{1,0:T(2,128)} %bitcast.11, f32[2,384]{1,0:T(2,128)} %bitcast.12, ...), custom_call_target="tpu_custom_call" | custom-call | tf_op jit(solution)/shard_map/pallas_call | solution.py:833
  95.9 0.0 copy-start.1
  95.9 1.9 %copy.16 = bf16[384,512]{1,0:T(8,128)(2,1)} copy(bf16[384,512]{1,0:T(8,128)(2,1)} %get-tuple-element.16) | data formatting | bytes 786432
  97.8 0.0 copy-start
  97.8 2.4 %copy.17 = bf16[1,2048,256]{2,1,0:T(8,128)(2,1)} copy(bf16[1,2048,256]{2,1,0:T(8,128)(2,1)} %bitcast.9) | data formatting | bytes 2097152
  100.2 0.0 copy-done.1
  100.2 1.0 copy.18
  101.1 0.0 copy-done
  101.1 1.0 copy.19
Async XLA Ops:
  95.9 4.2 %copy-start.1 = (bf16[2048,256]{1,0:T(8,128)(2,1)S(1)}, bf16[2048,256]{1,0:T(8,128)(2,1)}, u32[]{:S(2)}) copy-start(bf16[2048,256]{1,0:T(8,128)(2,1)} %get-tuple-element.10) | copy-start | bytes 3145732
  97.8 3.3 %copy-start = (bf16[2048,256]{1,0:T(8,128)(2,1)S(1)}, bf16[2048,256]{1,0:T(8,128)(2,1)}, u32[]{:S(2)}) copy-start(bf16[2048,256]{1,0:T(8,128)(2,1)} %get-tuple-element.11) | copy-start | bytes 3145732

commit v2 on v1

--- a/solution.py
+++ b/solution.py
@@ -10,6 +10,7 @@
 MESH = pl.DeviceIdType.MESH
 BF16 = jnp.bfloat16
 F32 = jnp.float32
+scope = jax.named_scope
 
 
 def each(count, step):
@@ -495,7 +496,8 @@
     far_base = lax.rem(own_base + 2, 4)
     bases = (own_base, far_base)
 
-    small[0].wait()
+    with scope("small_0_wait"):
+        small[0].wait()
     first, second = id_rows[0:1, :], id_rows[1:2, :]
     members = [(first >= b) & (first < b + 2) for b in bases]
     square = (tok_rows, tok_rows)
@@ -506,7 +508,8 @@
     kept = [m & (r < capacity) for m, r in zip(members, ranks)]
     seat = [jnp.where(k, r.astype(jnp.int32), -1) for k, r in zip(kept, ranks)]
 
-    small[1].wait()
+    with scope("small_1_wait"):
+        small[1].wait()
 
     def fill(i):
         one_hot = jnp.where(ints((lanes, tok_rows), 0) == seat[i], 1.0, 0.0)
@@ -523,7 +526,8 @@
         return rcopy(piece.at[t, 2], piece.at[t, 3], sl_s.at[3], sl_r.at[3], "fs", fs_at(1))
 
     fill(1)
-    pl.semaphore_wait(barrier, 3 + 3 + 1)
+    with scope("pl_semaphore_wait_barrier_3_3_1"):
+        pl.semaphore_wait(barrier, 3 + 3 + 1)
     slot_copy(2).start()
     piece[t, 0] = fill(0)
     slot_copy(1).start()
@@ -577,12 +581,14 @@
         rows = w_out[m].at[w_rows(fs_at(k), other_grp)]
         return rcopy(rows, rows, wy_s.at[m, k], wy_r.at[m, k], "grp", other_grp)
 
-    small[2].wait()
+    with scope("small_2_wait"):
+        small[2].wait()
     gain_col[...] = jnp.transpose(jnp.broadcast_to(gain[...], (8, block)))[:, 0:1]
     far_gain = gain_col[pl.ds(g * share, share), :]
 
     def send_far(m, k):
-        far_load(m, k).wait()
+        with scope("far_load_m_k_wait"):
+            far_load(m, k).wait()
         values = raw_far[m, k - 1]
         if m < 2:
             values = far_gain * values
@@ -590,19 +596,20 @@
         wz_copy(m, k).start()
 
     def round_own(m):
-        own_load(m).wait()
+        with scope("own_load_m_wait"):
+            own_load(m).wait()
         values = raw_own[m]
         if m < 2:
             values = gain_col[...] * values
         w_out[m][pl.ds(f * block, block), :] = values.astype(BF16)
 
-    for k in (1, 2, 3):
+    for k in (2, 3):
         send_far(2, k)
-    for m in (0, 1):
-        send_far(m, 1)
-
-    small[3].wait()
-    small[4].wait()
+
+    with scope("small_3_wait"):
+        small[3].wait()
+    with scope("small_4_wait"):
+        small[4].wait()
     group_exp = jnp.exp(group_logits[...])
     group_sum = jnp.sum(group_exp, axis=0, keepdims=True)
     pair_exp = jnp.exp(pair_logits[...])
@@ -630,62 +637,75 @@
     for k in (1, 2, 3):
         wm_copy(k).start()
 
-    for i in range(2):
-        back_place[i] = jnp.transpose(place[i].astype(F32))[:, 0:cap].astype(BF16)
+    def slot_arrival(k):
+        return rcopy(slots.at[0], piece.at[t, k], sl_s.at[k], sl_r.at[k], "fs", fs_at(k))
+
+    with scope("cross"):
+        slot_arrival(2).wait_recv()
+    relay_copy().start()
+    spread(2)
+    send_far(2, 1)
+    for k in (1, 2, 3):
+        for m in (0, 1):
+            send_far(m, k)
+
+    def hand_over(k):
+        with scope("hand%d" % k):
+            tx_arrival(k).wait_recv()
+        tf_copy(k).start()
+
+    def forward(m, k):
+        with scope("forward%d%d" % (m, k)):
+            wz_arrival(m, k).wait_recv()
+        wy_copy(m, k).start()
+
+    def arrived(m, k):
+        with scope("arrived%d%d" % (m, k)):
+            wy_arrival(m, k).wait_recv()
+
+    def land(k):
+        with scope("land%d" % k):
+            slot_arrival(k).wait_recv()
+        spread(k)
 
     def seat_weights(k, rows):
         cols = jnp.transpose(rows)
         wcol[k] = jnp.where(lax.rem(f, 2) == 0, cols[0:cap, 0:1], cols[0:cap, 1:2])
 
+    hand_over(0)
+    round_own(2)
+    for i in range(2):
+        back_place[i] = jnp.transpose(place[i].astype(F32))[:, 0:cap].astype(BF16)
     seat_weights(0, wsend[0])
-    round_own(2)
-
-    def slot_arrival(k):
-        return rcopy(slots.at[0], piece.at[t, k], sl_s.at[k], sl_r.at[k], "fs", fs_at(k))
-
-    slot_arrival(2).wait_recv()
-    relay_copy().start()
-    spread(2)
-    for k in (2, 3):
-        for m in (0, 1):
-            send_far(m, k)
+    land(1)
+    forward(2, 2)
+    forward(2, 3)
+    hand_over(2)
+    land(3)
+    forward(2, 1)
+    hand_over(1)
     for m in (0, 1):
         round_own(m)
-    slot_arrival(1).wait_recv()
-    spread(1)
-
-    def hand_over(k):
-        tx_arrival(k).wait_recv()
-        tf_copy(k).start()
-
-    hand_over(0)
-    for k in (1, 2, 3):
-        wz_arrival(2, k).wait_recv()
-        wy_copy(2, k).start()
-    hand_over(2)
-    hand_over(1)
-    slot_arrival(3).wait_recv()
-    spread(3)
+    forward(0, 1)
+    forward(1, 1)
+    hand_over(3)
 
     def dw_copy(j):
         src = down_out.at[pl.ds(tp_at(j) * block, block)]
         return rcopy(src, dwn.at[j], dw_s.at[j], dw_r.at[j], "tp", tp_at(j))
 
-    for k in (1, 2, 3):
-        wy_arrival(2, k).wait_recv()
-    for j in (1, 2, 3):
+    for k in (2, 3, 1):
+        arrived(2, k)
+    for j in (3, 2, 1):
         dw_copy(j).start()
-    for k in (1, 2, 3):
-        wm_copy(k).wait_recv()
-        seat_weights(k, wrecv[k])
-
-    for m in (0, 1):
-        wz_arrival(m, 1).wait_recv()
-        wy_copy(m, 1).start()
-    hand_over(3)
-    for k in (0, 2, 1, 3):
-        td_arrival(k).wait_recv()
-        tf_arrival(k).wait_recv()
+    with scope("weights_in"):
+        for k in (1, 2, 3):
+            wm_copy(k).wait_recv()
+            seat_weights(k, wrecv[k])
+    with scope("rows_in"):
+        for k in (0, 2, 1, 3):
+            td_arrival(k).wait_recv()
+            tf_arrival(k).wait_recv()
 
     def products(k, source):
         rows = piece[source, k]
@@ -707,21 +727,22 @@
             return c
         return step
 
-    lax.fori_loop(0, n_fs, first_products, 0)
+    with scope("products0"):
+        lax.fori_loop(0, n_fs, first_products, 0)
+    forward(0, 2)
+    forward(1, 2)
     for m in (0, 1):
-        wz_arrival(m, 2).wait_recv()
-        wy_copy(m, 2).start()
+        arrived(m, 1)
+    with scope("products1"):
+        lax.fori_loop(0, n_fs, more_products(1), 0)
+    forward(0, 3)
     for m in (0, 1):
-        wy_arrival(m, 1).wait_recv()
-    lax.fori_loop(0, n_fs, more_products(1), 0)
+        arrived(m, 2)
+    with scope("products2"):
+        lax.fori_loop(0, n_fs, more_products(2), 0)
+    forward(1, 3)
     for m in (0, 1):
-        wz_arrival(m, 3).wait_recv()
-        wy_copy(m, 3).start()
-    for m in (0, 1):
-        wy_arrival(m, 2).wait_recv()
-    lax.fori_loop(0, n_fs, more_products(2), 0)
-    for m in (0, 1):
-        wy_arrival(m, 3).wait_recv()
+        arrived(m, 3)
 
     def h_copy(j, k, ssem, rsem, source):
         return rcopy(hid.at[source, k], hid.at[source ^ j, k], ssem.at[k], rsem.at[k], "tp", tp_at(j))
@@ -735,57 +756,75 @@
     def hf_copy(k):
         return h_copy(1, k, hf_s, hf_r, 2)
 
-    order = (3, 2, 1, 0)
-    for k in order:
-        gate, up = products(k, fs_at(3))
-        gate = acc[0, k] + gate
-        up = acc[1, k] + up
-        hid[0, k] = (gate / (1.0 + jnp.exp(-gate)) * up * wcol[k]).astype(BF16)
-        hx_copy(k).start()
-        hd_copy(k).start()
-
-    for j in (1, 2, 3):
-        dw_copy(j).wait_recv()
-
-    def pass_on(k):
-        hx_copy(k).wait_recv()
+    for k in (3, 2, 1, 0):
+        with scope("hidden%d" % k):
+            gate, up = products(k, fs_at(3))
+            gate = acc[0, k] + gate
+            up = acc[1, k] + up
+            hid[0, k] = (gate / (1.0 + jnp.exp(-gate)) * up * wcol[k]).astype(BF16)
+            hx_copy(k).start()
+            hd_copy(k).start()
+
+    with scope("dw"):
+        for j in (1, 2, 3):
+            dw_copy(j).wait_recv()
+
+    def ready(k):
+        with scope("hx%d" % k):
+            hx_copy(k).wait_recv()
         hf_copy(k).start()
-
-    def result(k):
-        hd_copy(k).wait_recv()
-        hf_copy(k).wait_recv()
+        with scope("hf%d" % k):
+            hd_copy(k).wait_recv()
+            hf_copy(k).wait_recv()
+
+    halves = part_send.shape[1]
+    strip = width // halves
+
+    def result(k, c):
         total = None
         for j in range(n_tp):
-            rows = down_out[pl.ds(t * block, block), :] if j == 0 else dwn[j]
+            if j == 0:
+                rows = down_out[pl.ds(t * block + c * strip, strip), :]
+            else:
+                rows = dwn[j, c * strip : (c + 1) * strip, :]
             term = lax.dot_general(hid[j, k], rows, (((1,), (1,)), ((), ())), preferred_element_type=F32)
             total = term if total is None else total + term
         return total
 
-    def part_copy(i):
-        return rcopy(part_send.at[i], part_recv.at[i], pt_s.at[i], pt_r.at[i], "fs", fs_at(1))
-
-    def home_copy():
-        return rcopy(home_send, home, hm_s.at[0], hm_r.at[0], "fs", fs_at(2))
-
-    pass_on(3)
-    part_send[0] = result(3).astype(BF16)
-    part_copy(0).start()
-    pass_on(2)
-    keep[...] = result(2)
-    pass_on(1)
-    part_send[1] = result(1).astype(BF16)
-    part_copy(0).wait_recv()
-    home_send[...] = (keep[...] + part_recv[0].astype(F32)).astype(BF16)
-    home_copy().start()
-    part_copy(1).start()
-    pass_on(0)
-    keep[...] = result(0)
-    part_copy(1).wait_recv()
-    own_home[...] = (keep[...] + part_recv[1].astype(F32)).astype(BF16)
-    mix[...] = jnp.dot(back_place[0], own_home[...], preferred_element_type=F32)
-    home_copy().wait_recv()
-    far = jnp.dot(back_place[1], home[...], preferred_element_type=F32)
-    mixed[...] = (mix[...] + far).astype(BF16)
+    def part_copy(i, c):
+        return rcopy(part_send.at[i, c], part_recv.at[i, c], pt_s.at[i, c], pt_r.at[i, c], "fs", fs_at(1))
+
+    def home_copy(c):
+        return rcopy(home_send.at[c], home.at[c], hm_s.at[c], hm_r.at[c], "fs", fs_at(2))
+
+    strips = range(halves)
+    for i, (ours, theirs) in enumerate(((3, 2), (1, 0))):
+        ready(ours)
+        for c in strips:
+            part_send[i, c] = result(ours, c).astype(BF16)
+            part_copy(i, c).start()
+        if i == 0:
+            ready(theirs)
+            for c in strips:
+                keep[c] = result(theirs, c)
+    for c in strips:
+        with scope("part0%d" % c):
+            part_copy(0, c).wait_recv()
+        home_send[c] = (keep[c] + part_recv[0, c].astype(F32)).astype(BF16)
+        home_copy(c).start()
+    ready(0)
+    for c in strips:
+        keep[c] = result(0, c)
+    for c in strips:
+        with scope("part1%d" % c):
+            part_copy(1, c).wait_recv()
+        own_home[c] = (keep[c] + part_recv[1, c].astype(F32)).astype(BF16)
+        mix[c] = jnp.dot(back_place[0], own_home[c], preferred_element_type=F32)
+    for c in strips:
+        with scope("home%d" % c):
+            home_copy(c).wait_recv()
+        far = jnp.dot(back_place[1], home[c], preferred_element_type=F32)
+        mixed[:, c * strip : (c + 1) * strip] = (mix[c] + far).astype(BF16)
 
     for k in (1, 2):
         slot_copy(k).wait_send()
@@ -803,9 +842,10 @@
         hx_copy(k).wait_send()
         hd_copy(k).wait_send()
         hf_copy(k).wait_send()
-    for i in range(2):
-        part_copy(i).wait_send()
-    home_copy().wait_send()
+    for c in strips:
+        for i in range(2):
+            part_copy(i, c).wait_send()
+        home_copy(c).wait_send()
 
 
 def pair_body(
@@ -819,16 +859,18 @@
     cap = -(-capacity // 16) * 16
     lanes = -(-cap // 128) * 128
     vmem = pl.BlockSpec(memory_space=pltpu.VMEM)
-    hbm = pl.BlockSpec(memory_space=pl.ANY)
+    hbm = pl.BlockSpec(memory_space=pltpu.HBM)
     dma = pltpu.SemaphoreType.DMA
     matrix = jax.ShapeDtypeStruct((n_fs * block, hid), BF16)
     rows = (cap, width)
+    halves = 2
+    strips = (halves, cap, width // halves)
     sem_shapes = [
         (5,), (3, n_fs),
         (n_fs,), (n_fs,), (n_fs,), (n_fs,), (3, n_fs), (3, n_fs), (3, n_fs), (3, n_fs),
         (n_fs,), (n_fs,), (n_fs,), (n_fs,), (n_fs,), (n_fs,),
         (n_tp,), (n_tp,), (n_fs,), (n_fs,), (n_fs,), (n_fs,), (n_fs,), (n_fs,),
-        (2,), (2,), (1,), (1,),
+        (2, halves), (2, halves), (halves,), (halves,),
     ]
     mixed, *matrices = pl.pallas_call(
         functools.partial(pair_kernel, n_grp, n_fs, n_tp, capacity),
@@ -855,22 +897,50 @@
             pltpu.VMEM((2, n_fs, cap, hid), F32),
             pltpu.VMEM((n_tp, n_fs, cap, hid), BF16),
             pltpu.VMEM((n_tp, block, hid), BF16),
-            pltpu.VMEM((2, *rows), BF16),
-            pltpu.VMEM((2, *rows), BF16),
-            pltpu.VMEM(rows, F32),
-            pltpu.VMEM(rows, BF16),
-            pltpu.VMEM(rows, BF16),
-            pltpu.VMEM(rows, BF16),
-            pltpu.VMEM((tok_rows, width), F32),
+            pltpu.VMEM((2, *strips), BF16),
+            pltpu.VMEM((2, *strips), BF16),
+            pltpu.VMEM(strips, F32),
+            pltpu.VMEM(strips, BF16),
+            pltpu.VMEM(strips, BF16),
+            pltpu.VMEM(strips, BF16),
+            pltpu.VMEM((halves, tok_rows, width // halves), F32),
         ] + [dma(s) for s in sem_shapes],
         compiler_params=pltpu.CompilerParams(
-            collective_id=0, has_side_effects=True, vmem_limit_bytes=56 * 1024 * 1024
+            collective_id=0, has_side_effects=True, vmem_limit_bytes=40 * 1024 * 1024
         ),
-    )(
+    )(*(pltpu.with_memory_space_constraint(x, pltpu.HBM) for x in (
         tokens, norm_gain[None, :], expert_ids.T, group_logits.T, pair_logits.T,
         gate_weight, up_weight, down_weight,
-    )
-    return (mixed, *(m[None] for m in matrices))
+    )))
+    return write_out(mixed, *matrices)
+
+
+def write_kernel(mixed, gate, up, down, *rest):
+    outs, sem = rest[:4], rest[4]
+    copies = [
+        pltpu.make_async_copy(src, dst, sem.at[i])
+        for i, (src, dst) in enumerate(zip(
+            (gate, up, down, mixed), (outs[1].at[0], outs[2].at[0], outs[3].at[0], outs[0])
+        ))
+    ]
+    for copy in copies:
+        copy.start()
+    for copy in copies:
+        copy.wait()
+
+
+def write_out(mixed, *matrices):
+    return pl.pallas_call(
+        write_kernel,
+        out_shape=(
+            jax.ShapeDtypeStruct(mixed.shape, BF16),
+            *(jax.ShapeDtypeStruct((1, *m.shape), BF16) for m in matrices),
+        ),
+        in_specs=[pl.BlockSpec(memory_space=pltpu.VMEM)] * 4,
+        out_specs=(pl.BlockSpec(memory_space=pltpu.HBM),) * 4,
+        scratch_shapes=[pltpu.SemaphoreType.DMA((4,))],
+        compiler_params=pltpu.CompilerParams(vmem_limit_bytes=1024 * 1024),
+    )(mixed, *matrices)
 
 
 def paired(mesh, tokens, gate_weight, expert_ids, group_logits):

time: 102 us -> 86.5 us (0.85); the launches traced: 102 us -> 85.5 us
  Pallas kernels: 95.3 us -> 84.9 us
  local copies, waits for them, and re-layouts: 6.15 us -> 0 us
    pallas_call x1, Pallas kernels: 95.3 us -> 83 us  [pair_body(): pl.pallas_call(functools.partial(pair_kernel, n_grp, n_fs, n_tp, capacity...]
    unnamed x8 -> x0, local copies, waits for them, and re-layouts: 6.15 us -> none
    pallas_call x0 -> x1, Pallas kernels: none -> 1.82 us  [write_out(): pl.pallas_call(write_kernel, out_shape=(jax.ShapeDtypeStruct(mixed.shape,...]
where the time goes in v2:
time: 86.5 us; the launch traced here: 85.5 us
  Pallas kernels  84.9 us (98%)
    pallas_call x1, Pallas kernels, pair_body(): pl.pallas_call(functools.partial(pair_kernel, n_grp, n_fs, n_tp, capacity...  83 us
    pallas_call x1, Pallas kernels, write_out(): pl.pallas_call(write_kernel, out_shape=(jax.ShapeDtypeStruct(mixed.shape,...  1.82 us

profile of v2, /device:TPU:0, one launch (start us, length us, event | category | flops | bytes accessed | tf_op | source)
XLA Modules:
  0.0 85.5 jit_solution(16512226621259660310)
XLA Ops:
  0.6 83.0 %shard_map.111 = (bf16[384,512]{1,0:T(8,128)(2,1)S(1)}, bf16[2048,256]{1,0:T(8,128)(2,1)S(1)}, bf16[2048,256]{1,0:T(8,128)(2,1)S(1)}, bf16[2048,256]{1,0:T(8,128)(2,1)S(1)}) custom-call(bf16[384,512]{1,0:T(8,128)(2,1)} %tokens_in.1, f32[1,512]{1,0:T(1,128)} %bitcast.7, s32[2,384]{1,0:T(2,128)} %bitcast.4, f32[2,384]{1,0:T(2,128)} %bitcast.5, ...), custom_call_target="tpu_custom_call" | custom-call | tf_op jit(solution)/shard_map/pallas_call | solution.py:875
  83.7 1.8 %shard_map.112 = (bf16[384,512]{1,0:T(8,128)(2,1)}, bf16[1,2048,256]{2,1,0:T(8,128)(2,1)}, bf16[1,2048,256]{2,1,0:T(8,128)(2,1)}, bf16[1,2048,256]{2,1,0:T(8,128)(2,1)}) custom-call(bf16[384,512]{1,0:T(8,128)(2,1)S(1)} %get-tuple-element.8.mixed, bf16[2048,256]{1,0:T(8,128)(2,1)S(1)} %get-tuple-element.9.gate, bf16[2048,256]{1,0:T(8,128)(2,1)S(1)} %get-tuple-element.10.up, ...), custom_call_target="tpu_custom_call" | custom-call | tf_op jit(solution)/shard_map/pallas_call | solution.py:933

commit v3 on v2

--- a/solution.py
+++ b/solution.py
@@ -418,15 +418,14 @@
 
 
 def pair_kernel(
-    n_grp, n_fs, n_tp, capacity,
+    n_grp, n_fs, n_tp, capacity, chunk,
     tokens_in, gain_in, ids_in, group_in, pair_in, gate_in, up_in, down_in,
     mixed, gate_out, up_out, down_out,
     tokens, gain, id_rows, group_logits, pair_logits, gain_col,
     raw_own, raw_far, cast, slots, place, back_place, wsend, wrecv, wcol,
-    piece, acc, hid, dwn, part_send, part_recv, keep, home_send, home, own_home, mix,
-    in_sem, raw_sem,
-    sl_s, sl_r, wm_s, wm_r, wz_s, wz_r, wy_s, wy_r, tx_s, tx_r, td_s, td_r, tf_s, tf_r,
-    dw_s, dw_r, hx_s, hx_r, hd_s, hd_r, hf_s, hf_r, pt_s, pt_r, hm_s, hm_r,
+    piece, acc, hid, dwn, part_send, part_recv, keep, home_send, back, mix,
+    in_sem, raw_sem, send, sl_r, wm_r, wz_r, wy_r, tx_r, td_r, tf_r,
+    dw_r, hx_r, hd_r, hf_r, pt_r, hm_r,
 ):
     g, f, t = lax.axis_index("grp"), lax.axis_index("fs"), lax.axis_index("tp")
     cap, width = piece.shape[2], piece.shape[3]
@@ -436,11 +435,18 @@
     lanes = place.shape[1]
     pair = n_fs // 2
 
+    inner = (f == 1) | (f == 2)
+
     def flip(i, k):
         return (i, i + 1 - 2 * lax.rem(i, 2), lax.rem(i + 2, 4), 3 - i)[k]
 
     def fs_at(k):
-        return flip(f, k)
+        if isinstance(k, int):
+            return flip(f, k)
+        return jnp.where(k == 1, flip(f, 1), jnp.where(k == 2, flip(f, 2), flip(f, 3)))
+
+    def by_role(at_inner, at_outer):
+        return jnp.where(inner, at_inner, at_outer)
 
     def tp_at(j):
         return flip(t, j)
@@ -452,6 +458,12 @@
             src_ref=src, dst_ref=dst, send_sem=ssem, recv_sem=rsem,
             device_id={axis: peer}, device_id_type=MESH,
         )
+
+    def all_sent(index, ref):
+        rcopy(ref, ref, send.at[index], send.at[index], "fs", fs_at(1)).wait_send()
+
+    def all_here(sem, ref):
+        rcopy(ref, ref, sem, sem, "fs", fs_at(1)).wait_recv()
 
     small = [
         pltpu.make_async_copy(src, dst, in_sem.at[i])
@@ -520,10 +532,10 @@
 
     def slot_copy(k):
         src = slots.at[0] if k == 1 else slots.at[1]
-        return rcopy(src, piece.at[t, k], sl_s.at[k], sl_r.at[k], "fs", fs_at(k))
+        return rcopy(src, piece.at[t, k], send.at[0], sl_r.at[k], "fs", fs_at(k))
 
     def relay_copy():
-        return rcopy(piece.at[t, 2], piece.at[t, 3], sl_s.at[3], sl_r.at[3], "fs", fs_at(1))
+        return rcopy(piece.at[t, 2], piece.at[t, 3], send.at[0], sl_r.at[3], "fs", fs_at(1))
 
     fill(1)
     with scope("pl_semaphore_wait_barrier_3_3_1"):
@@ -534,27 +546,27 @@
 
     def tx_copy(k):
         src = piece.at[t, k]
-        return rcopy(src, src, tx_s.at[k], tx_r.at[k], "tp", tp_at(2))
+        return rcopy(src, src, send.at[1], tx_r.at[k], "tp", tp_at(2))
 
     def td_copy(k):
         src = piece.at[t, k]
-        return rcopy(src, src, td_s.at[k], td_r.at[k], "tp", tp_at(1))
+        return rcopy(src, src, send.at[2], td_r.at[k // 3], "tp", tp_at(1))
 
     def tf_copy(k):
         src = piece.at[tp_at(2), k]
-        return rcopy(src, src, tf_s.at[k], tf_r.at[k], "tp", tp_at(1))
+        return rcopy(src, src, send.at[3], tf_r.at[k // 3], "tp", tp_at(1))
 
     def tx_arrival(k):
         src = piece.at[tp_at(2), k]
-        return rcopy(src, src, tx_s.at[k], tx_r.at[k], "tp", tp_at(2))
+        return rcopy(src, src, send.at[1], tx_r.at[k], "tp", tp_at(2))
 
     def td_arrival(k):
         src = piece.at[tp_at(1), k]
-        return rcopy(src, src, td_s.at[k], td_r.at[k], "tp", tp_at(1))
+        return rcopy(src, src, send.at[2], td_r.at[k // 3], "tp", tp_at(1))
 
     def tf_arrival(k):
         src = piece.at[tp_at(3), k]
-        return rcopy(src, src, tf_s.at[k], tf_r.at[k], "tp", tp_at(1))
+        return rcopy(src, src, send.at[3], tf_r.at[k // 3], "tp", tp_at(1))
 
     def spread(k):
         tx_copy(k).start()
@@ -562,27 +574,32 @@
 
     spread(0)
 
-    def w_rows(source, part):
-        return pl.ds(source * block + part * share, share)
-
-    def wz_copy(m, k):
-        return rcopy(cast.at[m, k - 1], w_out[m].at[w_rows(f, g)],
-                     wz_s.at[m, k], wz_r.at[m, k], "fs", fs_at(k))
-
-    def wz_arrival(m, k):
-        return rcopy(cast.at[m, k - 1], w_out[m].at[w_rows(fs_at(k), g)],
-                     wz_s.at[m, k], wz_r.at[m, k], "fs", fs_at(k))
-
-    def wy_copy(m, k):
-        rows = w_out[m].at[w_rows(fs_at(k), g)]
-        return rcopy(rows, rows, wy_s.at[m, k], wy_r.at[m, k], "grp", other_grp)
-
-    def wy_arrival(m, k):
-        rows = w_out[m].at[w_rows(fs_at(k), other_grp)]
-        return rcopy(rows, rows, wy_s.at[m, k], wy_r.at[m, k], "grp", other_grp)
-
-    with scope("small_2_wait"):
-        small[2].wait()
+    half = share // wz_r.shape[2]
+    halves = range(wz_r.shape[2])
+
+    def w_rows(source, part, h):
+        return pl.ds(source * block + part * share + h * half, half)
+
+    def wz_copy(m, k, h):
+        return rcopy(cast.at[m, k - 1, pl.ds(h * half, half)], w_out[m].at[w_rows(f, g, h)],
+                     send.at[4], wz_r.at[m, k - 1, h], "fs", fs_at(k))
+
+    def wz_arrival(m, k, h):
+        return rcopy(cast.at[m, k - 1, pl.ds(h * half, half)], w_out[m].at[w_rows(fs_at(k), g, h)],
+                     send.at[4], wz_r.at[m, k - 1, h], "fs", fs_at(k))
+
+    def wy_sem(m, k):
+        return wy_r.at[0] if m == 2 else wy_r.at[k]
+
+    def wy_copy(m, k, h):
+        rows = w_out[m].at[w_rows(fs_at(k), g, h)]
+        return rcopy(rows, rows, send.at[5], wy_sem(m, k), "grp", other_grp)
+
+    def wy_arrival(m, k, h):
+        rows = w_out[m].at[w_rows(fs_at(k), other_grp, h)]
+        return rcopy(rows, rows, send.at[5], wy_sem(m, k), "grp", other_grp)
+
+    small[2].wait()
     gain_col[...] = jnp.transpose(jnp.broadcast_to(gain[...], (8, block)))[:, 0:1]
     far_gain = gain_col[pl.ds(g * share, share), :]
 
@@ -593,7 +610,8 @@
         if m < 2:
             values = far_gain * values
         cast[m, k - 1] = values.astype(BF16)
-        wz_copy(m, k).start()
+        for h in halves:
+            wz_copy(m, k, h).start()
 
     def round_own(m):
         with scope("own_load_m_wait"):
@@ -603,7 +621,7 @@
             values = gain_col[...] * values
         w_out[m][pl.ds(f * block, block), :] = values.astype(BF16)
 
-    for k in (2, 3):
+    for k in (1, 2, 3):
         send_far(2, k)
 
     with scope("small_3_wait"):
@@ -617,7 +635,7 @@
     group_count = group_exp.shape[0]
 
     def wm_copy(k):
-        return rcopy(wsend.at[k // 2], wrecv.at[k], wm_s.at[k], wm_r.at[k], "fs", fs_at(k))
+        return rcopy(wsend.at[k // 2], wrecv.at[k], send.at[6], wm_r.at[0], "fs", fs_at(k))
 
     chosen = jnp.zeros_like(group_sum)
     for i in range(group_count):
@@ -638,13 +656,12 @@
         wm_copy(k).start()
 
     def slot_arrival(k):
-        return rcopy(slots.at[0], piece.at[t, k], sl_s.at[k], sl_r.at[k], "fs", fs_at(k))
+        return rcopy(slots.at[0], piece.at[t, k], send.at[0], sl_r.at[k], "fs", fs_at(k))
 
     with scope("cross"):
         slot_arrival(2).wait_recv()
     relay_copy().start()
     spread(2)
-    send_far(2, 1)
     for k in (1, 2, 3):
         for m in (0, 1):
             send_far(m, k)
@@ -655,13 +672,14 @@
         tf_copy(k).start()
 
     def forward(m, k):
-        with scope("forward%d%d" % (m, k)):
-            wz_arrival(m, k).wait_recv()
-        wy_copy(m, k).start()
-
-    def arrived(m, k):
-        with scope("arrived%d%d" % (m, k)):
-            wy_arrival(m, k).wait_recv()
+        for h in halves:
+            with scope("forward%d" % m):
+                wz_arrival(m, k, h).wait_recv()
+            wy_copy(m, k, h).start()
+
+    def arrived(k):
+        with scope("arrived"):
+            all_here(wy_r.at[k], gate_out.at[pl.ds(0, 2 * share)])
 
     def land(k):
         with scope("land%d" % k):
@@ -678,34 +696,34 @@
         back_place[i] = jnp.transpose(place[i].astype(F32))[:, 0:cap].astype(BF16)
     seat_weights(0, wsend[0])
     land(1)
-    forward(2, 2)
-    forward(2, 3)
+    for k in (2, 1, 3):
+        forward(2, k)
     hand_over(2)
-    land(3)
-    forward(2, 1)
     hand_over(1)
     for m in (0, 1):
         round_own(m)
-    forward(0, 1)
-    forward(1, 1)
-    hand_over(3)
 
     def dw_copy(j):
         src = down_out.at[pl.ds(tp_at(j) * block, block)]
-        return rcopy(src, dwn.at[j], dw_s.at[j], dw_r.at[j], "tp", tp_at(j))
-
-    for k in (2, 3, 1):
-        arrived(2, k)
+        return rcopy(src, dwn.at[j], send.at[7], dw_r.at[0], "tp", tp_at(j))
+
+    with scope("down_in"):
+        all_here(wy_r.at[0], down_out.at[pl.ds(0, 3 * share)])
     for j in (3, 2, 1):
         dw_copy(j).start()
+    turns = (by_role(1, 2), by_role(2, 1), 3)
+    for m in (0, 1):
+        forward(m, turns[0])
+    land(3)
+    for m in (0, 1):
+        forward(m, turns[1])
     with scope("weights_in"):
+        all_here(wm_r.at[0], wrecv.at[pl.ds(1, 3)])
         for k in (1, 2, 3):
-            wm_copy(k).wait_recv()
             seat_weights(k, wrecv[k])
     with scope("rows_in"):
-        for k in (0, 2, 1, 3):
-            td_arrival(k).wait_recv()
-            tf_arrival(k).wait_recv()
+        all_here(td_r.at[0], piece.at[t, pl.ds(0, 3)])
+        all_here(tf_r.at[0], piece.at[t, pl.ds(0, 3)])
 
     def products(k, source):
         rows = piece[source, k]
@@ -727,125 +745,163 @@
             return c
         return step
 
-    with scope("products0"):
-        lax.fori_loop(0, n_fs, first_products, 0)
-    forward(0, 2)
-    forward(1, 2)
+    def multiply(step, blocks):
+        with scope("products"):
+            lax.fori_loop(*blocks, step, 0)
+
+    first = (0, n_fs - 1)
+    multiply(first_products, first)
+    arrived(turns[0])
+    multiply(more_products(turns[0]), first)
     for m in (0, 1):
-        arrived(m, 1)
-    with scope("products1"):
-        lax.fori_loop(0, n_fs, more_products(1), 0)
-    forward(0, 3)
-    for m in (0, 1):
-        arrived(m, 2)
-    with scope("products2"):
-        lax.fori_loop(0, n_fs, more_products(2), 0)
-    forward(1, 3)
-    for m in (0, 1):
-        arrived(m, 3)
-
-    def h_copy(j, k, ssem, rsem, source):
-        return rcopy(hid.at[source, k], hid.at[source ^ j, k], ssem.at[k], rsem.at[k], "tp", tp_at(j))
-
-    def hx_copy(k):
-        return h_copy(2, k, hx_s, hx_r, 0)
-
-    def hd_copy(k):
-        return h_copy(1, k, hd_s, hd_r, 0)
-
-    def hf_copy(k):
-        return h_copy(1, k, hf_s, hf_r, 2)
-
-    for k in (3, 2, 1, 0):
-        with scope("hidden%d" % k):
-            gate, up = products(k, fs_at(3))
+        forward(m, turns[2])
+    hand_over(3)
+    with scope("rows_in"):
+        all_here(td_r.at[1], piece.at[t, 3])
+        all_here(tf_r.at[1], piece.at[t, 3])
+    first_products(3, 0)
+    more_products(turns[0])(3, 0)
+    arrived(turns[1])
+    multiply(more_products(turns[1]), (0, n_fs))
+    arrived(turns[2])
+
+    spans = [pl.ds(at, min(chunk, cap - at)) for at in range(0, cap, chunk)]
+    parts = range(len(spans))
+
+    def h_copy(j, k, c, ssem, rsem, source):
+        src, dst = hid.at[source, k, spans[c]], hid.at[source ^ j, k, spans[c]]
+        return rcopy(src, dst, ssem, rsem, "tp", tp_at(j))
+
+    def hx_copy(k, c):
+        return h_copy(2, k, c, send.at[8], hx_r.at[k, c], 0)
+
+    def hd_copy(k, c):
+        return h_copy(1, k, c, send.at[9], hd_r.at[k], 0)
+
+    def hf_copy(k, c):
+        return h_copy(1, k, c, send.at[10], hf_r.at[k, c], 2)
+
+    last = fs_at(turns[2])
+    blocks = (by_role(2, 3), by_role(3, 2), 1, 0)
+    for k in blocks:
+        with scope("hidden"):
+            gate, up = products(k, last)
             gate = acc[0, k] + gate
             up = acc[1, k] + up
             hid[0, k] = (gate / (1.0 + jnp.exp(-gate)) * up * wcol[k]).astype(BF16)
-            hx_copy(k).start()
-            hd_copy(k).start()
-
-    with scope("dw"):
-        for j in (1, 2, 3):
-            dw_copy(j).wait_recv()
-
-    def ready(k):
-        with scope("hx%d" % k):
-            hx_copy(k).wait_recv()
-        hf_copy(k).start()
-        with scope("hf%d" % k):
-            hd_copy(k).wait_recv()
-            hf_copy(k).wait_recv()
-
-    halves = part_send.shape[1]
-    strip = width // halves
-
-    def result(k, c):
-        total = None
-        for j in range(n_tp):
-            if j == 0:
-                rows = down_out[pl.ds(t * block + c * strip, strip), :]
-            else:
-                rows = dwn[j, c * strip : (c + 1) * strip, :]
-            term = lax.dot_general(hid[j, k], rows, (((1,), (1,)), ((), ())), preferred_element_type=F32)
-            total = term if total is None else total + term
+            for c in parts:
+                hx_copy(k, c).start()
+                hd_copy(k, c).start()
+
+    with scope("drain"):
+        all_here(dw_r.at[0], dwn.at[pl.ds(1, 3)])
+        all_sent(0, piece.at[t, pl.ds(0, 3)])
+        for i in (1, 2, 3):
+            all_sent(i, piece.at[t])
+        all_sent(4, cast)
+        all_sent(5, cast)
+        all_sent(6, wrecv.at[pl.ds(1, 3)])
+        all_sent(7, dwn.at[pl.ds(1, 3)])
+
+    queue = [(k, c) for k in blocks for c in parts]
+
+    def pass_on(n):
+        if n < len(queue):
+            with scope("hx"):
+                hx_copy(*queue[n]).wait_recv()
+            hf_copy(*queue[n]).start()
+
+    def result(n):
+        k, c = queue[n]
+
+        def term(j):
+            rows = down_out[pl.ds(t * block, block), :] if j == 0 else dwn[j]
+            return lax.dot_general(
+                hid[j, k, spans[c], :], rows, (((1,), (1,)), ((), ())), preferred_element_type=F32)
+
+        if c == 0:
+            with scope("hd"):
+                all_here(hd_r.at[k], hid.at[1, k])
+        total = term(0) + term(1)
+        if n == 0:
+            pass_on(0)
+        total = total + term(2)
+        if n > 0:
+            pass_on(n + 1)
+        with scope("hf"):
+            hf_copy(k, c).wait_recv()
+        total = total + term(3)
+        if n == 0:
+            pass_on(1)
         return total
 
     def part_copy(i, c):
-        return rcopy(part_send.at[i, c], part_recv.at[i, c], pt_s.at[i, c], pt_r.at[i, c], "fs", fs_at(1))
-
-    def home_copy(c):
-        return rcopy(home_send.at[c], home.at[c], hm_s.at[c], hm_r.at[c], "fs", fs_at(2))
-
-    strips = range(halves)
-    for i, (ours, theirs) in enumerate(((3, 2), (1, 0))):
-        ready(ours)
-        for c in strips:
-            part_send[i, c] = result(ours, c).astype(BF16)
-            part_copy(i, c).start()
-        if i == 0:
-            ready(theirs)
-            for c in strips:
-                keep[c] = result(theirs, c)
-    for c in strips:
-        with scope("part0%d" % c):
-            part_copy(0, c).wait_recv()
-        home_send[c] = (keep[c] + part_recv[0, c].astype(F32)).astype(BF16)
-        home_copy(c).start()
-    ready(0)
-    for c in strips:
-        keep[c] = result(0, c)
-    for c in strips:
-        with scope("part1%d" % c):
-            part_copy(1, c).wait_recv()
-        own_home[c] = (keep[c] + part_recv[1, c].astype(F32)).astype(BF16)
-        mix[c] = jnp.dot(back_place[0], own_home[c], preferred_element_type=F32)
-    for c in strips:
-        with scope("home%d" % c):
-            home_copy(c).wait_recv()
-        far = jnp.dot(back_place[1], home[c], preferred_element_type=F32)
-        mixed[:, c * strip : (c + 1) * strip] = (mix[c] + far).astype(BF16)
-
-    for k in (1, 2):
-        slot_copy(k).wait_send()
-    relay_copy().wait_send()
-    for k in (1, 2, 3):
-        wm_copy(k).wait_send()
-        dw_copy(k).wait_send()
-        for m in range(3):
-            wz_copy(m, k).wait_send()
-            wy_copy(m, k).wait_send()
-    for k in range(n_fs):
-        tx_copy(k).wait_send()
-        td_copy(k).wait_send()
-        tf_copy(k).wait_send()
-        hx_copy(k).wait_send()
-        hd_copy(k).wait_send()
-        hf_copy(k).wait_send()
-    for c in strips:
-        for i in range(2):
-            part_copy(i, c).wait_send()
-        home_copy(c).wait_send()
+        return rcopy(part_send.at[i, spans[c]], part_recv.at[i, spans[c]],
+                     send.at[11 + i // 2], pt_r.at[i, c], "fs", fs_at(1))
+
+    def home_copy(i, c):
+        return rcopy(home_send.at[i, spans[c]], back.at[1, spans[c]],
+                     send.at[13], hm_r.at[0], "fs", fs_at(2 + i))
+
+    def home_step(n):
+        if n < 0 or n >= 2 * len(parts):
+            return
+        i, c = divmod(n, len(parts))
+
+        @pl.when(inner)
+        def _():
+            with scope("part%d" % i):
+                part_copy(i, c).wait_recv()
+            both = keep[i, spans[c], :] + part_recv[i, spans[c], :].astype(F32)
+            home_send[i, spans[c], :] = both.astype(BF16)
+            home_copy(i, c).start()
+
+    for n in range(len(queue)):
+        i, c = divmod(n, len(parts))
+        if i == 2:
+            part_send[2, spans[c], :] = result(n).astype(BF16)
+            part_copy(2, c).start()
+        else:
+            keep[min(i, 2), spans[c], :] = result(n)
+        if i < 2:
+            @pl.when(jnp.logical_not(inner))
+            def _():
+                part_send[i, spans[c], :] = keep[i, spans[c], :].astype(BF16)
+                part_copy(i, c).start()
+        home_step(n - 2)
+
+    def finish_own():
+        for c in parts:
+            with scope("part2"):
+                part_copy(2, c).wait_recv()
+            both = keep[2, spans[c], :] + part_recv[2, spans[c], :].astype(F32)
+            back[0, spans[c], :] = both.astype(BF16)
+
+    def finish_far():
+        with scope("home"):
+            all_here(hm_r.at[0], back.at[1])
+
+    pl.when(inner)(finish_own)
+    pl.when(jnp.logical_not(inner))(finish_far)
+    sooner, later = by_role(0, 1), by_role(1, 0)
+    mix[...] = jnp.dot(back_place[sooner], back[sooner], preferred_element_type=F32)
+    pl.when(inner)(finish_far)
+    pl.when(jnp.logical_not(inner))(finish_own)
+    with scope("last_dot"):
+        more = jnp.dot(back_place[later], back[later], preferred_element_type=F32)
+        mixed[...] = (mix[...] + more).astype(BF16)
+
+    for i in (8, 9, 10):
+        all_sent(i, hid.at[0])
+    all_sent(12, part_send.at[2])
+
+    @pl.when(inner)
+    def _():
+        all_sent(13, home_send)
+
+    @pl.when(jnp.logical_not(inner))
+    def _():
+        all_sent(11, part_send.at[pl.ds(0, 2)])
 
 
 def pair_body(
@@ -863,17 +919,14 @@
     dma = pltpu.SemaphoreType.DMA
     matrix = jax.ShapeDtypeStruct((n_fs * block, hid), BF16)
     rows = (cap, width)
-    halves = 2
-    strips = (halves, cap, width // halves)
+    chunk = -(-cap // 32) * 16
+    spans = -(-cap // chunk)
     sem_shapes = [
-        (5,), (3, n_fs),
-        (n_fs,), (n_fs,), (n_fs,), (n_fs,), (3, n_fs), (3, n_fs), (3, n_fs), (3, n_fs),
-        (n_fs,), (n_fs,), (n_fs,), (n_fs,), (n_fs,), (n_fs,),
-        (n_tp,), (n_tp,), (n_fs,), (n_fs,), (n_fs,), (n_fs,), (n_fs,), (n_fs,),
-        (2, halves), (2, halves), (halves,), (halves,),
+        (5,), (3, n_fs), (14,), (n_fs,), (1,), (3, n_fs - 1, 2), (n_fs,), (n_fs,), (2,), (2,),
+        (1,), (n_fs, spans), (n_fs,), (n_fs, spans), (3, spans), (1,),
     ]
     mixed, *matrices = pl.pallas_call(
-        functools.partial(pair_kernel, n_grp, n_fs, n_tp, capacity),
+        functools.partial(pair_kernel, n_grp, n_fs, n_tp, capacity, chunk),
         out_shape=(jax.ShapeDtypeStruct((tok_rows, width), BF16), matrix, matrix, matrix),
         in_specs=[hbm] * 8,
         out_specs=(vmem,) * 4,
@@ -897,13 +950,12 @@
             pltpu.VMEM((2, n_fs, cap, hid), F32),
             pltpu.VMEM((n_tp, n_fs, cap, hid), BF16),
             pltpu.VMEM((n_tp, block, hid), BF16),
-            pltpu.VMEM((2, *strips), BF16),
-            pltpu.VMEM((2, *strips), BF16),
-            pltpu.VMEM(strips, F32),
-            pltpu.VMEM(strips, BF16),
-            pltpu.VMEM(strips, BF16),
-            pltpu.VMEM(strips, BF16),
-            pltpu.VMEM((halves, tok_rows, width // halves), F32),
+            pltpu.VMEM((3, *rows), BF16),
+            pltpu.VMEM((3, *rows), BF16),
+            pltpu.VMEM((3, *rows), F32),
+            pltpu.VMEM((2, *rows), BF16),
+            pltpu.VMEM((2, *rows), BF16),
+            pltpu.VMEM((tok_rows, width), F32),
         ] + [dma(s) for s in sem_shapes],
         compiler_params=pltpu.CompilerParams(
             collective_id=0, has_side_effects=True, vmem_limit_bytes=40 * 1024 * 1024

time: 86.5 us -> 80.7 us (0.933); the launches traced: 85.5 us -> 80.6 us
  Pallas kernels: 84.9 us -> 79.9 us
    pallas_call x1, Pallas kernels: 83 us -> 78.1 us  [pair_body(): pl.pallas_call(functools.partial(pair_kernel, n_grp, n_fs, n_tp, capacity...]
where the time goes in v3:
time: 80.7 us; the launch traced here: 80.6 us
  Pallas kernels  79.9 us (99%)
    pallas_call x1, Pallas kernels, pair_body(): pl.pallas_call(functools.partial(pair_kernel, n_grp, n_fs, n_tp, capacity...  78.1 us
    pallas_call x1, Pallas kernels, write_out(): pl.pallas_call(write_kernel, out_shape=(jax.ShapeDtypeStruct(mixed.shape,...  1.82 us

profile of v3, /device:TPU:0, one launch (start us, length us, event | category | flops | bytes accessed | tf_op | source)
XLA Modules:
  0.0 80.6 jit_solution(10032984460683838867)
XLA Ops:
  0.6 78.1 %shard_map.111 = (bf16[384,512]{1,0:T(8,128)(2,1)S(1)}, bf16[2048,256]{1,0:T(8,128)(2,1)S(1)}, bf16[2048,256]{1,0:T(8,128)(2,1)S(1)}, bf16[2048,256]{1,0:T(8,128)(2,1)S(1)}) custom-call(bf16[384,512]{1,0:T(8,128)(2,1)} %tokens_in.1, f32[1,512]{1,0:T(1,128)} %bitcast.7, s32[2,384]{1,0:T(2,128)} %bitcast.4, f32[2,384]{1,0:T(2,128)} %bitcast.5, ...), custom_call_target="tpu_custom_call" | custom-call | tf_op jit(solution)/shard_map/pallas_call | solution.py:928
  78.7 1.8 %shard_map.112 = (bf16[384,512]{1,0:T(8,128)(2,1)}, bf16[1,2048,256]{2,1,0:T(8,128)(2,1)}, bf16[1,2048,256]{2,1,0:T(8,128)(2,1)}, bf16[1,2048,256]{2,1,0:T(8,128)(2,1)}) custom-call(bf16[384,512]{1,0:T(8,128)(2,1)S(1)} %get-tuple-element.8.mixed, bf16[2048,256]{1,0:T(8,128)(2,1)S(1)} %get-tuple-element.9.gate, bf16[2048,256]{1,0:T(8,128)(2,1)S(1)} %get-tuple-element.10.up, ...), custom_call_target="tpu_custom_call" | custom-call | tf_op jit(solution)/shard_map/pallas_call | solution.py:985

commit v4 on v3

--- a/solution.py
+++ b/solution.py
@@ -424,7 +424,7 @@
     tokens, gain, id_rows, group_logits, pair_logits, gain_col,
     raw_own, raw_far, cast, slots, place, back_place, wsend, wrecv, wcol,
     piece, acc, hid, dwn, part_send, part_recv, keep, home_send, back, mix,
-    in_sem, raw_sem, send, sl_r, wm_r, wz_r, wy_r, tx_r, td_r, tf_r,
+    in_sem, raw_sem, send, sl_r, wm_r, wd_r, wz_r, wy_r, tx_r, td_r, tf_r,
     dw_r, hx_r, hd_r, hf_r, pt_r, hm_r,
 ):
     g, f, t = lax.axis_index("grp"), lax.axis_index("fs"), lax.axis_index("tp")
@@ -477,8 +477,12 @@
 
     def far_load(m, k):
         return pltpu.make_async_copy(
-            w_in[m].at[fs_at(k), pl.ds(g * share, share)], raw_far.at[m, k - 1], raw_sem.at[m, k]
+            w_in[m].at[fs_at(k), pl.ds(g * share, share)], raw_far.at[m, k - 1], raw_sem.at[m, 1]
         )
+
+    def far_loaded(m):
+        whole = w_in[m].at[pl.ds(0, 3), pl.ds(0, share)]
+        pltpu.make_async_copy(whole, raw_far.at[m], raw_sem.at[m, 1]).wait()
 
     def own_load(m):
         return pltpu.make_async_copy(w_in[m].at[f], raw_own.at[m], raw_sem.at[m, 0])
@@ -500,6 +504,42 @@
         greet("fs", fs_at(k))
         greet("tp", tp_at(k))
     greet("grp", other_grp)
+
+    cuts = wz_r.shape[2]
+
+    def cuts_of(m):
+        return range(1 if m == 2 else cuts)
+
+    def piece_rows(m):
+        return share if m == 2 else share // cuts
+
+    def w_rows(source, part, m, h):
+        return pl.ds(source * block + part * share + h * piece_rows(m), piece_rows(m))
+
+    def far_rows(m, k, h):
+        return cast.at[m, k - 1, pl.ds(h * piece_rows(m), piece_rows(m))]
+
+    def wz_sem(m, k, h):
+        return wd_r.at[k - 1] if m == 2 else wz_r.at[m, k - 1, h]
+
+    def wz_copy(m, k, h):
+        return rcopy(far_rows(m, k, h), w_out[m].at[w_rows(f, g, m, h)],
+                     send.at[2], wz_sem(m, k, h), "fs", fs_at(k))
+
+    def wz_arrival(m, k, h):
+        return rcopy(far_rows(m, k, h), w_out[m].at[w_rows(fs_at(k), g, m, h)],
+                     send.at[2], wz_sem(m, k, h), "fs", fs_at(k))
+
+    def wy_sem(m, k):
+        return wy_r.at[0] if m == 2 else wy_r.at[k]
+
+    def wy_copy(m, k, h):
+        rows = w_out[m].at[w_rows(fs_at(k), g, m, h)]
+        return rcopy(rows, rows, send.at[2], wy_sem(m, k), "grp", other_grp)
+
+    def wy_arrival(m, k, h):
+        rows = w_out[m].at[w_rows(fs_at(k), other_grp, m, h)]
+        return rcopy(rows, rows, send.at[2], wy_sem(m, k), "grp", other_grp)
 
     def ints(shape, axis):
         return lax.broadcasted_iota(jnp.int32, shape, axis)
@@ -538,7 +578,7 @@
         return rcopy(piece.at[t, 2], piece.at[t, 3], send.at[0], sl_r.at[3], "fs", fs_at(1))
 
     fill(1)
-    with scope("pl_semaphore_wait_barrier_3_3_1"):
+    with scope("barrier"):
         pl.semaphore_wait(barrier, 3 + 3 + 1)
     slot_copy(2).start()
     piece[t, 0] = fill(0)
@@ -550,11 +590,11 @@
 
     def td_copy(k):
         src = piece.at[t, k]
-        return rcopy(src, src, send.at[2], td_r.at[k // 3], "tp", tp_at(1))
+        return rcopy(src, src, send.at[1], td_r.at[k // 3], "tp", tp_at(1))
 
     def tf_copy(k):
         src = piece.at[tp_at(2), k]
-        return rcopy(src, src, send.at[3], tf_r.at[k // 3], "tp", tp_at(1))
+        return rcopy(src, src, send.at[1], tf_r.at[k // 3], "tp", tp_at(1))
 
     def tx_arrival(k):
         src = piece.at[tp_at(2), k]
@@ -562,11 +602,11 @@
 
     def td_arrival(k):
         src = piece.at[tp_at(1), k]
-        return rcopy(src, src, send.at[2], td_r.at[k // 3], "tp", tp_at(1))
+        return rcopy(src, src, send.at[1], td_r.at[k // 3], "tp", tp_at(1))
 
     def tf_arrival(k):
         src = piece.at[tp_at(3), k]
-        return rcopy(src, src, send.at[3], tf_r.at[k // 3], "tp", tp_at(1))
+        return rcopy(src, src, send.at[1], tf_r.at[k // 3], "tp", tp_at(1))
 
     def spread(k):
         tx_copy(k).start()
@@ -574,43 +614,14 @@
 
     spread(0)
 
-    half = share // wz_r.shape[2]
-    halves = range(wz_r.shape[2])
-
-    def w_rows(source, part, h):
-        return pl.ds(source * block + part * share + h * half, half)
-
-    def wz_copy(m, k, h):
-        return rcopy(cast.at[m, k - 1, pl.ds(h * half, half)], w_out[m].at[w_rows(f, g, h)],
-                     send.at[4], wz_r.at[m, k - 1, h], "fs", fs_at(k))
-
-    def wz_arrival(m, k, h):
-        return rcopy(cast.at[m, k - 1, pl.ds(h * half, half)], w_out[m].at[w_rows(fs_at(k), g, h)],
-                     send.at[4], wz_r.at[m, k - 1, h], "fs", fs_at(k))
-
-    def wy_sem(m, k):
-        return wy_r.at[0] if m == 2 else wy_r.at[k]
-
-    def wy_copy(m, k, h):
-        rows = w_out[m].at[w_rows(fs_at(k), g, h)]
-        return rcopy(rows, rows, send.at[5], wy_sem(m, k), "grp", other_grp)
-
-    def wy_arrival(m, k, h):
-        rows = w_out[m].at[w_rows(fs_at(k), other_grp, h)]
-        return rcopy(rows, rows, send.at[5], wy_sem(m, k), "grp", other_grp)
-
     small[2].wait()
     gain_col[...] = jnp.transpose(jnp.broadcast_to(gain[...], (8, block)))[:, 0:1]
     far_gain = gain_col[pl.ds(g * share, share), :]
 
     def send_far(m, k):
         with scope("far_load_m_k_wait"):
-            far_load(m, k).wait()
-        values = raw_far[m, k - 1]
-        if m < 2:
-            values = far_gain * values
-        cast[m, k - 1] = values.astype(BF16)
-        for h in halves:
+            cast[m, k - 1] = (far_gain * raw_far[m, k - 1]).astype(BF16)
+        for h in cuts_of(m):
             wz_copy(m, k, h).start()
 
     def round_own(m):
@@ -621,8 +632,12 @@
             values = gain_col[...] * values
         w_out[m][pl.ds(f * block, block), :] = values.astype(BF16)
 
+    far_loaded(2)
     for k in (1, 2, 3):
-        send_far(2, k)
+        cast[2, k - 1] = raw_far[2, k - 1].astype(BF16)
+        wz_copy(2, k, 0).start()
+    far_loaded(0)
+    far_loaded(1)
 
     with scope("small_3_wait"):
         small[3].wait()
@@ -635,7 +650,7 @@
     group_count = group_exp.shape[0]
 
     def wm_copy(k):
-        return rcopy(wsend.at[k // 2], wrecv.at[k], send.at[6], wm_r.at[0], "fs", fs_at(k))
+        return rcopy(wsend.at[k // 2], wrecv.at[k], send.at[3], wm_r.at[0], "fs", fs_at(k))
 
     chosen = jnp.zeros_like(group_sum)
     for i in range(group_count):
@@ -671,11 +686,21 @@
             tx_arrival(k).wait_recv()
         tf_copy(k).start()
 
-    def forward(m, k):
-        for h in halves:
-            with scope("forward%d" % m):
-                wz_arrival(m, k, h).wait_recv()
-            wy_copy(m, k, h).start()
+    def forward(m, k, h):
+        with scope("forward%d%d%d" % (m, k, h)):
+            wz_arrival(m, k, h).wait_recv()
+        wy_copy(m, k, h).start()
+
+    def forward_all(steps, more):
+        @pl.when(inner)
+        def _():
+            for step in steps:
+                forward(*step)
+
+        @pl.when(jnp.logical_not(inner))
+        def _():
+            for step in more:
+                forward(*step)
 
     def arrived(k):
         with scope("arrived"):
@@ -697,7 +722,7 @@
     seat_weights(0, wsend[0])
     land(1)
     for k in (2, 1, 3):
-        forward(2, k)
+        forward(2, k, 0)
     hand_over(2)
     hand_over(1)
     for m in (0, 1):
@@ -705,18 +730,19 @@
 
     def dw_copy(j):
         src = down_out.at[pl.ds(tp_at(j) * block, block)]
-        return rcopy(src, dwn.at[j], send.at[7], dw_r.at[0], "tp", tp_at(j))
+        return rcopy(src, dwn.at[j], send.at[4], dw_r.at[0], "tp", tp_at(j))
 
     with scope("down_in"):
         all_here(wy_r.at[0], down_out.at[pl.ds(0, 3 * share)])
     for j in (3, 2, 1):
         dw_copy(j).start()
+    def steps(*turns):
+        return [(m, k, h) for k in turns for m in (0, 1) for h in cuts_of(m)]
+
     turns = (by_role(1, 2), by_role(2, 1), 3)
-    for m in (0, 1):
-        forward(m, turns[0])
+    forward_all(steps(1), steps(2))
     land(3)
-    for m in (0, 1):
-        forward(m, turns[1])
+    forward_all(steps(2), steps(1))
     with scope("weights_in"):
         all_here(wm_r.at[0], wrecv.at[pl.ds(1, 3)])
         for k in (1, 2, 3):
@@ -753,8 +779,7 @@
     multiply(first_products, first)
     arrived(turns[0])
     multiply(more_products(turns[0]), first)
-    for m in (0, 1):
-        forward(m, turns[2])
+    forward_all(steps(3), steps(3))
     hand_over(3)
     with scope("rows_in"):
         all_here(td_r.at[1], piece.at[t, 3])
@@ -773,16 +798,16 @@
         return rcopy(src, dst, ssem, rsem, "tp", tp_at(j))
 
     def hx_copy(k, c):
-        return h_copy(2, k, c, send.at[8], hx_r.at[k, c], 0)
+        return h_copy(2, k, c, send.at[5], hx_r.at[k, c], 0)
 
     def hd_copy(k, c):
-        return h_copy(1, k, c, send.at[9], hd_r.at[k], 0)
+        return h_copy(1, k, c, send.at[5], hd_r.at[k], 0)
 
     def hf_copy(k, c):
-        return h_copy(1, k, c, send.at[10], hf_r.at[k, c], 2)
+        return h_copy(1, k, c, send.at[5], hf_r.at[k, c], 2)
 
     last = fs_at(turns[2])
-    blocks = (by_role(2, 3), by_role(3, 2), 1, 0)
+    blocks = (by_role(1, 3), 2, by_role(3, 1), 0)
     for k in blocks:
         with scope("hidden"):
             gate, up = products(k, last)
@@ -796,12 +821,10 @@
     with scope("drain"):
         all_here(dw_r.at[0], dwn.at[pl.ds(1, 3)])
         all_sent(0, piece.at[t, pl.ds(0, 3)])
-        for i in (1, 2, 3):
-            all_sent(i, piece.at[t])
-        all_sent(4, cast)
-        all_sent(5, cast)
-        all_sent(6, wrecv.at[pl.ds(1, 3)])
-        all_sent(7, dwn.at[pl.ds(1, 3)])
+        all_sent(1, piece.at[pl.ds(0, 3)])
+        all_sent(2, raw_far)
+        all_sent(3, wrecv.at[pl.ds(1, 3)])
+        all_sent(4, dwn.at[pl.ds(1, 3)])
 
     queue = [(k, c) for k in blocks for c in parts]
 
@@ -837,11 +860,11 @@
 
     def part_copy(i, c):
         return rcopy(part_send.at[i, spans[c]], part_recv.at[i, spans[c]],
-                     send.at[11 + i // 2], pt_r.at[i, c], "fs", fs_at(1))
+                     send.at[6 + i // 2], pt_r.at[i, c], "fs", fs_at(1))
 
     def home_copy(i, c):
         return rcopy(home_send.at[i, spans[c]], back.at[1, spans[c]],
-                     send.at[13], hm_r.at[0], "fs", fs_at(2 + i))
+                     send.at[8], hm_r.at[0], "fs", fs_at(2 + i))
 
     def home_step(n):
         if n < 0 or n >= 2 * len(parts):
@@ -852,29 +875,29 @@
         def _():
             with scope("part%d" % i):
                 part_copy(i, c).wait_recv()
-            both = keep[i, spans[c], :] + part_recv[i, spans[c], :].astype(F32)
+            both = keep[i + 1, spans[c], :] + part_recv[i, spans[c], :].astype(F32)
             home_send[i, spans[c], :] = both.astype(BF16)
             home_copy(i, c).start()
 
     for n in range(len(queue)):
         i, c = divmod(n, len(parts))
-        if i == 2:
-            part_send[2, spans[c], :] = result(n).astype(BF16)
-            part_copy(2, c).start()
-        else:
-            keep[min(i, 2), spans[c], :] = result(n)
-        if i < 2:
-            @pl.when(jnp.logical_not(inner))
-            def _():
-                part_send[i, spans[c], :] = keep[i, spans[c], :].astype(BF16)
-                part_copy(i, c).start()
-        home_step(n - 2)
+        keep[i, spans[c], :] = result(n)
+
+        def send_part(to):
+            part_send[to, spans[c], :] = keep[i, spans[c], :].astype(BF16)
+            part_copy(to, c).start()
+
+        if i < 3:
+            pl.when(jnp.logical_not(inner))(functools.partial(send_part, i))
+        if i == 0:
+            pl.when(inner)(functools.partial(send_part, 2))
+        home_step(n - len(parts) - 1)
 
     def finish_own():
         for c in parts:
             with scope("part2"):
                 part_copy(2, c).wait_recv()
-            both = keep[2, spans[c], :] + part_recv[2, spans[c], :].astype(F32)
+            both = keep[3, spans[c], :] + part_recv[2, spans[c], :].astype(F32)
             back[0, spans[c], :] = both.astype(BF16)
 
     def finish_far():
@@ -891,17 +914,16 @@
         more = jnp.dot(back_place[later], back[later], preferred_element_type=F32)
         mixed[...] = (mix[...] + more).astype(BF16)
 
-    for i in (8, 9, 10):
-        all_sent(i, hid.at[0])
-    all_sent(12, part_send.at[2])
+    all_sent(5, hid.at[pl.ds(0, 3)])
+    all_sent(7, part_send.at[2])
 
     @pl.when(inner)
     def _():
-        all_sent(13, home_send)
+        all_sent(8, home_send)
 
     @pl.when(jnp.logical_not(inner))
     def _():
-        all_sent(11, part_send.at[pl.ds(0, 2)])
+        all_sent(6, part_send.at[pl.ds(0, 2)])
 
 
 def pair_body(
@@ -919,10 +941,10 @@
     dma = pltpu.SemaphoreType.DMA
     matrix = jax.ShapeDtypeStruct((n_fs * block, hid), BF16)
     rows = (cap, width)
-    chunk = -(-cap // 32) * 16
+    chunk = -(-cap // 48) * 16
     spans = -(-cap // chunk)
     sem_shapes = [
-        (5,), (3, n_fs), (14,), (n_fs,), (1,), (3, n_fs - 1, 2), (n_fs,), (n_fs,), (2,), (2,),
+        (5,), (3, 2), (9,), (n_fs,), (1,), (n_fs - 1,), (2, n_fs - 1, 4), (n_fs,), (n_fs,), (2,), (2,),
         (1,), (n_fs, spans), (n_fs,), (n_fs, spans), (3, spans), (1,),
     ]
     mixed, *matrices = pl.pallas_call(
@@ -952,7 +974,7 @@
             pltpu.VMEM((n_tp, block, hid), BF16),
             pltpu.VMEM((3, *rows), BF16),
             pltpu.VMEM((3, *rows), BF16),
-            pltpu.VMEM((3, *rows), F32),
+            pltpu.VMEM((n_fs, *rows), F32),
             pltpu.VMEM((2, *rows), BF16),
             pltpu.VMEM((2, *rows), BF16),
             pltpu.VMEM((tok_rows, width), F32),
@@ -969,16 +991,16 @@
 
 def write_kernel(mixed, gate, up, down, *rest):
     outs, sem = rest[:4], rest[4]
-    copies = [
-        pltpu.make_async_copy(src, dst, sem.at[i])
-        for i, (src, dst) in enumerate(zip(
-            (gate, up, down, mixed), (outs[1].at[0], outs[2].at[0], outs[3].at[0], outs[0])
-        ))
-    ]
-    for copy in copies:
-        copy.start()
-    for copy in copies:
-        copy.wait()
+    pairs = (
+        (gate, outs[1].at[0]), (up, outs[2].at[0]), (down, outs[3].at[0]), (mixed, outs[0])
+    )
+    for i, (src, dst) in enumerate(pairs):
+        rows = src.shape[0] // 4
+        for c in range(4):
+            at = pl.ds(c * rows, rows)
+            pltpu.make_async_copy(src.at[at], dst.at[at], sem.at[i]).start()
+    for i, (src, dst) in enumerate(pairs):
+        pltpu.make_async_copy(src, dst, sem.at[i]).wait()
 
 
 def write_out(mixed, *matrices):

time: 80.7 us -> 78.4 us (0.971)
  Pallas kernels: 79.9 us -> 77.6 us
    pallas_call x1, Pallas kernels: 78.1 us -> 75.8 us  [pair_body(): pl.pallas_call(functools.partial(pair_kernel, n_grp, n_fs, n_tp, capacity...]
where the time goes in v4:
time: 78.4 us; the launch traced here: 78.2 us
  Pallas kernels  77.6 us (99%)
    pallas_call x1, Pallas kernels, pair_body(): pl.pallas_call(functools.partial(pair_kernel, n_grp, n_fs, n_tp, capacity...  75.8 us
    pallas_call x1, Pallas kernels, write_out(): pl.pallas_call(write_kernel, out_shape=(jax.ShapeDtypeStruct(mixed.shape,...  1.81 us

profile of v4, /device:TPU:0, one launch (start us, length us, event | category | flops | bytes accessed | tf_op | source)
XLA Modules:
  0.0 78.2 jit_solution(18428360820777386553)
XLA Ops:
  0.6 75.8 %shard_map.111 = (bf16[384,512]{1,0:T(8,128)(2,1)S(1)}, bf16[2048,256]{1,0:T(8,128)(2,1)S(1)}, bf16[2048,256]{1,0:T(8,128)(2,1)S(1)}, bf16[2048,256]{1,0:T(8,128)(2,1)S(1)}) custom-call(bf16[384,512]{1,0:T(8,128)(2,1)} %tokens_in.1, f32[1,512]{1,0:T(1,128)} %bitcast.7, s32[2,384]{1,0:T(2,128)} %bitcast.4, f32[2,384]{1,0:T(2,128)} %bitcast.5, ...), custom_call_target="tpu_custom_call" | custom-call | tf_op jit(solution)/shard_map/pallas_call | solution.py:950
  76.4 1.8 %shard_map.112 = (bf16[384,512]{1,0:T(8,128)(2,1)}, bf16[1,2048,256]{2,1,0:T(8,128)(2,1)}, bf16[1,2048,256]{2,1,0:T(8,128)(2,1)}, bf16[1,2048,256]{2,1,0:T(8,128)(2,1)}) custom-call(bf16[384,512]{1,0:T(8,128)(2,1)S(1)} %get-tuple-element.8.mixed, bf16[2048,256]{1,0:T(8,128)(2,1)S(1)} %get-tuple-element.9.gate, bf16[2048,256]{1,0:T(8,128)(2,1)S(1)} %get-tuple-element.10.up, ...), custom_call_target="tpu_custom_call" | custom-call | tf_op jit(solution)/shard_map/pallas_call | solution.py:1007

commit v5 on v4

--- a/solution.py
+++ b/solution.py
@@ -781,16 +781,18 @@
     multiply(more_products(turns[0]), first)
     forward_all(steps(3), steps(3))
     hand_over(3)
+    arrived(turns[1])
+    multiply(more_products(turns[1]), first)
     with scope("rows_in"):
         all_here(td_r.at[1], piece.at[t, 3])
         all_here(tf_r.at[1], piece.at[t, 3])
     first_products(3, 0)
     more_products(turns[0])(3, 0)
-    arrived(turns[1])
-    multiply(more_products(turns[1]), (0, n_fs))
+    more_products(turns[1])(3, 0)
     arrived(turns[2])
 
-    spans = [pl.ds(at, min(chunk, cap - at)) for at in range(0, cap, chunk)]
+    edges = (0, *chunk, cap)
+    spans = [pl.ds(a, b - a) for a, b in zip(edges, edges[1:])]
     parts = range(len(spans))
 
     def h_copy(j, k, c, ssem, rsem, source):
@@ -941,8 +943,8 @@
     dma = pltpu.SemaphoreType.DMA
     matrix = jax.ShapeDtypeStruct((n_fs * block, hid), BF16)
     rows = (cap, width)
-    chunk = -(-cap // 48) * 16
-    spans = -(-cap // chunk)
+    chunk = (cap // 80 * 16, cap // 80 * 16 * 2, cap // 80 * 16 * 3)
+    spans = len(chunk) + 1
     sem_shapes = [
         (5,), (3, 2), (9,), (n_fs,), (1,), (n_fs - 1,), (2, n_fs - 1, 4), (n_fs,), (n_fs,), (2,), (2,),
         (1,), (n_fs, spans), (n_fs,), (n_fs, spans), (3, spans), (1,),

time: 78.4 us -> 77.9 us (level)
  no operation moved by 1% of the time
where the time goes in v5:
time: 77.9 us; the launch traced here: 77.7 us
  Pallas kernels  77.1 us (99%)
    pallas_call x1, Pallas kernels, pair_body(): pl.pallas_call(functools.partial(pair_kernel, n_grp, n_fs, n_tp, capacity...  75.3 us
    pallas_call x1, Pallas kernels, write_out(): pl.pallas_call(write_kernel, out_shape=(jax.ShapeDtypeStruct(mixed.shape,...  1.81 us

profile of v5, /device:TPU:0, one launch (start us, length us, event | category | flops | bytes accessed | tf_op | source)
XLA Modules:
  0.0 77.7 jit_solution(15120729085549245527)
XLA Ops:
  0.6 75.3 %shard_map.111 = (bf16[384,512]{1,0:T(8,128)(2,1)S(1)}, bf16[2048,256]{1,0:T(8,128)(2,1)S(1)}, bf16[2048,256]{1,0:T(8,128)(2,1)S(1)}, bf16[2048,256]{1,0:T(8,128)(2,1)S(1)}) custom-call(bf16[384,512]{1,0:T(8,128)(2,1)} %tokens_in.1, f32[1,512]{1,0:T(1,128)} %bitcast.7, s32[2,384]{1,0:T(2,128)} %bitcast.4, f32[2,384]{1,0:T(2,128)} %bitcast.5, ...), custom_call_target="tpu_custom_call" | custom-call | tf_op jit(solution)/shard_map/pallas_call | solution.py:952
  75.9 1.8 %shard_map.112 = (bf16[384,512]{1,0:T(8,128)(2,1)}, bf16[1,2048,256]{2,1,0:T(8,128)(2,1)}, bf16[1,2048,256]{2,1,0:T(8,128)(2,1)}, bf16[1,2048,256]{2,1,0:T(8,128)(2,1)}) custom-call(bf16[384,512]{1,0:T(8,128)(2,1)S(1)} %get-tuple-element.8.mixed, bf16[2048,256]{1,0:T(8,128)(2,1)S(1)} %get-tuple-element.9.gate, bf16[2048,256]{1,0:T(8,128)(2,1)S(1)} %get-tuple-element.10.up, ...), custom_call_target="tpu_custom_call" | custom-call | tf_op jit(solution)/shard_map/pallas_call | solution.py:1009

commit v6 on v5

--- a/solution.py
+++ b/solution.py
@@ -810,14 +810,27 @@
 
     last = fs_at(turns[2])
     blocks = (by_role(1, 3), 2, by_role(3, 1), 0)
+    def diagonal_copy(k, c):
+        src, dst = hid.at[0, k, spans[c]], hid.at[3, k, spans[c]]
+        return rcopy(src, dst, send.at[5], hf_r.at[k, c], "tp", tp_at(3))
+
+    direct = 1
+
+    def launch(i):
+        for c in parts:
+            if i == 0 and c < direct:
+                diagonal_copy(blocks[i], c).start()
+            hx_copy(blocks[i], c).start()
+
     for k in blocks:
         with scope("hidden"):
             gate, up = products(k, last)
             gate = acc[0, k] + gate
             up = acc[1, k] + up
             hid[0, k] = (gate / (1.0 + jnp.exp(-gate)) * up * wcol[k]).astype(BF16)
+            if k is blocks[0]:
+                launch(0)
             for c in parts:
-                hx_copy(k, c).start()
                 hd_copy(k, c).start()
 
     with scope("drain"):
@@ -834,7 +847,8 @@
         if n < len(queue):
             with scope("hx"):
                 hx_copy(*queue[n]).wait_recv()
-            hf_copy(*queue[n]).start()
+            if n >= direct:
+                hf_copy(*queue[n]).start()
 
     def result(n):
         k, c = queue[n]
@@ -850,6 +864,7 @@
         total = term(0) + term(1)
         if n == 0:
             pass_on(0)
+            launch(1)
         total = total + term(2)
         if n > 0:
             pass_on(n + 1)
@@ -883,6 +898,8 @@
 
     for n in range(len(queue)):
         i, c = divmod(n, len(parts))
+        if c == 0 and i in (1, 2):
+            launch(i + 1)
         keep[i, spans[c], :] = result(n)
 
         def send_part(to):

time: 77.9 us -> 77.4 us (level)
  no operation moved by 1% of the time
where the time goes in v6:
time: 77.4 us; the launch traced here: 77.1 us
  Pallas kernels  76.5 us (99%)
    pallas_call x1, Pallas kernels, pair_body(): pl.pallas_call(functools.partial(pair_kernel, n_grp, n_fs, n_tp, capacity...  74.7 us
    pallas_call x1, Pallas kernels, write_out(): pl.pallas_call(write_kernel, out_shape=(jax.ShapeDtypeStruct(mixed.shape,...  1.81 us

profile of v6, /device:TPU:0, one launch (start us, length us, event | category | flops | bytes accessed | tf_op | source)
XLA Modules:
  0.0 77.1 jit_solution(17380746303725088662)
XLA Ops:
  0.6 74.7 %shard_map.111 = (bf16[384,512]{1,0:T(8,128)(2,1)S(1)}, bf16[2048,256]{1,0:T(8,128)(2,1)S(1)}, bf16[2048,256]{1,0:T(8,128)(2,1)S(1)}, bf16[2048,256]{1,0:T(8,128)(2,1)S(1)}) custom-call(bf16[384,512]{1,0:T(8,128)(2,1)} %tokens_in.1, f32[1,512]{1,0:T(1,128)} %bitcast.7, s32[2,384]{1,0:T(2,128)} %bitcast.4, f32[2,384]{1,0:T(2,128)} %bitcast.5, ...), custom_call_target="tpu_custom_call" | custom-call | tf_op jit(solution)/shard_map/pallas_call | solution.py:969
  75.3 1.8 %shard_map.112 = (bf16[384,512]{1,0:T(8,128)(2,1)}, bf16[1,2048,256]{2,1,0:T(8,128)(2,1)}, bf16[1,2048,256]{2,1,0:T(8,128)(2,1)}, bf16[1,2048,256]{2,1,0:T(8,128)(2,1)}) custom-call(bf16[384,512]{1,0:T(8,128)(2,1)S(1)} %get-tuple-element.8.mixed, bf16[2048,256]{1,0:T(8,128)(2,1)S(1)} %get-tuple-element.9.gate, bf16[2048,256]{1,0:T(8,128)(2,1)S(1)} %get-tuple-element.10.up, ...), custom_call_target="tpu_custom_call" | custom-call | tf_op jit(solution)/shard_map/pallas_call | solution.py:1026

commit v7 on v6

--- a/solution.py
+++ b/solution.py
@@ -864,7 +864,6 @@
         total = term(0) + term(1)
         if n == 0:
             pass_on(0)
-            launch(1)
         total = total + term(2)
         if n > 0:
             pass_on(n + 1)
@@ -872,6 +871,7 @@
             hf_copy(k, c).wait_recv()
         total = total + term(3)
         if n == 0:
+            launch(1)
             pass_on(1)
         return total
 

time: 77.4 us -> 77.3 us (level)
  no operation moved by 1% of the time
where the time goes in v7:
time: 77.3 us; the launch traced here: 76.9 us
  Pallas kernels  76.3 us (99%)
    pallas_call x1, Pallas kernels, pair_body(): pl.pallas_call(functools.partial(pair_kernel, n_grp, n_fs, n_tp, capacity...  74.5 us
    pallas_call x1, Pallas kernels, write_out(): pl.pallas_call(write_kernel, out_shape=(jax.ShapeDtypeStruct(mixed.shape,...  1.81 us

profile of v7, /device:TPU:0, one launch (start us, length us, event | category | flops | bytes accessed | tf_op | source)
XLA Modules:
  0.0 76.9 jit_solution(17358167898261094735)
XLA Ops:
  0.6 74.5 %shard_map.111 = (bf16[384,512]{1,0:T(8,128)(2,1)S(1)}, bf16[2048,256]{1,0:T(8,128)(2,1)S(1)}, bf16[2048,256]{1,0:T(8,128)(2,1)S(1)}, bf16[2048,256]{1,0:T(8,128)(2,1)S(1)}) custom-call(bf16[384,512]{1,0:T(8,128)(2,1)} %tokens_in.1, f32[1,512]{1,0:T(1,128)} %bitcast.7, s32[2,384]{1,0:T(2,128)} %bitcast.4, f32[2,384]{1,0:T(2,128)} %bitcast.5, ...), custom_call_target="tpu_custom_call" | custom-call | tf_op jit(solution)/shard_map/pallas_call | solution.py:969
  75.1 1.8 %shard_map.112 = (bf16[384,512]{1,0:T(8,128)(2,1)}, bf16[1,2048,256]{2,1,0:T(8,128)(2,1)}, bf16[1,2048,256]{2,1,0:T(8,128)(2,1)}, bf16[1,2048,256]{2,1,0:T(8,128)(2,1)}) custom-call(bf16[384,512]{1,0:T(8,128)(2,1)S(1)} %get-tuple-element.8.mixed, bf16[2048,256]{1,0:T(8,128)(2,1)S(1)} %get-tuple-element.9.gate, bf16[2048,256]{1,0:T(8,128)(2,1)S(1)} %get-tuple-element.10.up, ...), custom_call_target="tpu_custom_call" | custom-call | tf_op jit(solution)/shard_map/pallas_call | solution.py:1026
